TPU v7x, 256 devices: a whole 4x4x8 slice. The times are simulated.
256 devices in a mesh: sp: 16 (over y, x), tp: 16 (over z, core).
Axes of the slice: x: 4, y: 4, z: 8, core: 2. Of those that a mesh axis runs over, the one named last changes fastest.
Arguments:
- queries: bfloat16 [16384, 2048], P('sp', 'tp'), may hold values from -8 to 8
- keys: bfloat16 [16384, 512], P('sp'), may hold values from -6 to 6
- values: bfloat16 [16384, 512], P('sp'), may hold values from -6 to 6
- query_gain: float32 [2048], P('tp'), may hold values from 0.2 to 40
- key_gain: float32 [128], replicated, may hold values from 0.1 to 1.9
- out_weight: bfloat16 [2048, 2048], replicated, may hold values from -0.125 to 0.125
- residual: bfloat16 [16384, 2048], P(('sp', 'tp')), may hold values from -2 to 2
- norm_gain: float32 [2048], replicated, may hold values from 0.1 to 1.9
- route_experts: int32 [16384, 2], P(('sp', 'tp')), may hold values from 0 to 15, as said below
- expert_scores: float32 [16384, 2], P(('sp', 'tp')), may hold values from -9 to 9
- group_prob: float32 [16384], P(('sp', 'tp')), may hold values from 0.5 to 1
- w_gate: bfloat16 [16, 2048, 2048], P('sp', None, 'tp'), may hold values from -0.125 to 0.125
- w_up: bfloat16 [16, 2048, 2048], P('sp', None, 'tp'), may hold values from -0.125 to 0.125
- w_down: bfloat16 [16, 2048, 2048], P('sp', 'tp'), may hold values from -0.125 to 0.125
Outputs:
- mixed: bfloat16 [16384, 2048], P(('sp', 'tp'))
Inputs may be any that keep to these rules, and one draw needn't show every extreme that they name: `route_experts`: each row names 2 different experts of one group, expert e lying in group e // 8. In the rows of one device (aligned blocks of 64 rows) 5 * 8 rows choose one group and the others another; inside a group those rows are spread over its experts as evenly as whole numbers allow, so no expert is named by more than 10 rows of one device and some expert by exactly 10.
All inputs are finite; a program needn't handle non-finite values.
Results may differ from a plain program's by a relative error of at most 0.025.
Values may be sent and summed in bfloat16 or wider, within the bound.
No kernel may reach another device: no remote copies, remote signals or barrier semaphores. Data moves between devices by JAX's collectives and lax.ppermute only.
A program may use at most 128 MiB of HBM per device.

v0:
```python
import functools
import math

import jax
import jax.numpy as jnp
from jax import lax
from jax.experimental import pallas as pl
from jax.experimental.pallas import tpu as pltpu
from jax.sharding import Mesh
from jax.sharding import PartitionSpec as P

GRID_W = 64
HEAD = 128
SP = ("y", "x")
TP = ("z", "core")
SP_TP = ("y", "x", "z", "core")
rope_base = 10000.0
norm_eps = 1e-06
f32 = jnp.float32
bf16 = jnp.bfloat16


def room(mib):
    return pltpu.CompilerParams(vmem_limit_bytes=mib * 1024 * 1024)


def dot(a, b):
    return jnp.dot(a, b, preferred_element_type=f32)


def bundle_kernel(gate_ref, up_ref, down_ref, out_ref):
    units = gate_ref.shape[1]
    out_ref[0] = gate_ref[...]
    out_ref[1] = up_ref[...]
    for k in range(down_ref.shape[1] // HEAD):
        out_ref[2, k * units : (k + 1) * units, :] = down_ref[:, k * HEAD : (k + 1) * HEAD]


def bundle(gate, up, down):
    width, units = gate.shape
    rows = width // 2
    spec = pl.BlockSpec((rows, units), lambda i: (i, 0))
    return pl.pallas_call(
        bundle_kernel,
        grid=(2,),
        in_specs=[spec, spec, pl.BlockSpec((units, rows), lambda i: (0, i))],
        out_specs=pl.BlockSpec((3, rows, units), lambda i: (0, i, 0)),
        out_shape=jax.ShapeDtypeStruct((3, width, units), bf16),
        name="bundle",
    )(gate, up, down)


def prep_kernel(
    where_ref, q_ref, k_ref, v_ref, qg_ref, kg_ref, cos_ref, sin_ref, q_out, kv_a, kv_b
):
    lane = lax.broadcasted_iota(jnp.int32, (GRID_W, HEAD), 1)
    even = lane % 2 == 0
    from_row = lane < HEAD // 2
    col_cos = cos_ref[16:, :]
    col_sin = sin_ref[16:, :]

    def turn(vectors, gain, row_cos, row_sin):
        mean = jnp.mean(vectors * vectors, axis=-1, keepdims=True)
        u = vectors * lax.rsqrt(mean + norm_eps) * gain
        swapped = jnp.where(even, pltpu.roll(u, HEAD - 1, 1), pltpu.roll(u, 1, 1))
        cosine = jnp.where(from_row, row_cos, col_cos)
        sine = jnp.where(from_row, row_sin, col_sin)
        return u * cosine + swapped * sine

    for r in range(q_ref.shape[0] // GRID_W):
        rows = slice(r * GRID_W, (r + 1) * GRID_W)
        q_out[rows, :] = turn(
            q_ref[rows, :].astype(f32), qg_ref[...], cos_ref[r : r + 1, :], sin_ref[r : r + 1, :]
        ).astype(bf16)
    half = k_ref.shape[0] // GRID_W
    first = where_ref[0] * half
    for r in range(half):
        rows = slice(r * GRID_W, (r + 1) * GRID_W)
        row_cos = cos_ref[pl.ds(first + r, 1), :]
        row_sin = sin_ref[pl.ds(first + r, 1), :]
        kv_out = kv_a if r < half // 2 else kv_b
        at = r % (half // 2)
        rows_out = slice(at * GRID_W, (at + 1) * GRID_W)
        kv_out[rows_out, :HEAD] = turn(
            k_ref[rows, :].astype(f32), kg_ref[...], row_cos, row_sin
        ).astype(bf16)
        kv_out[rows_out, HEAD:] = v_ref[rows, :]


def prep(where, queries, keys, values, query_gain, key_gain, cosine, sine):
    tokens = queries.shape[0]
    half = tokens // 2
    whole = lambda shape: pl.BlockSpec(shape, lambda i, w: (0, 0))
    part = pl.BlockSpec((half, HEAD), lambda i, w: (w[0], w[1]))
    return pl.pallas_call(
        prep_kernel,
        grid_spec=pltpu.PrefetchScalarGridSpec(
            num_scalar_prefetch=1,
            grid=(1,),
            in_specs=[
                whole((tokens, HEAD)),
                part,
                part,
                whole((1, HEAD)),
                whole((1, HEAD)),
                whole(cosine.shape),
                whole(sine.shape),
            ],
            out_specs=[
                whole((tokens, HEAD)),
                whole((half // 2, 2 * HEAD)),
                whole((half // 2, 2 * HEAD)),
            ],
        ),
        out_shape=[
            jax.ShapeDtypeStruct((tokens, HEAD), bf16),
            jax.ShapeDtypeStruct((half // 2, 2 * HEAD), bf16),
            jax.ShapeDtypeStruct((half // 2, 2 * HEAD), bf16),
        ],
        name="prep",
    )(where, queries, keys, values, query_gain, key_gain, cosine, sine)


BQ = 256


def attend_kernel(first, last, count, where_ref, own_ref, sib_ref, *refs):
    kv_refs, refs = refs[:count], refs[count:]
    if not first:
        acc_in, top_in, *refs = refs
    out_a, out_b, kk, vv = refs
    rows = kv_refs[0].shape[0]

    @pl.when((pl.program_id(0) == 0) & (pl.program_id(1) == 0))
    def _():
        for b in range(count):
            span = slice(b * rows, (b + 1) * rows)
            k = kv_refs[b][:, :HEAD]
            kk[span, :HEAD] = k
            kk[span, HEAD:] = k
            vv[span, :HEAD] = kv_refs[b][:, HEAD:]
            vv[span, HEAD:] = jnp.ones((rows, HEAD), bf16)

    q = jnp.where(pl.program_id(0) == 0, own_ref[...].astype(f32), sib_ref[...].astype(f32))
    scaled = q * (HEAD ** (-0.5) * math.log2(math.e))
    high = scaled.astype(bf16)
    low = (scaled - high.astype(f32)).astype(bf16)
    pair = jnp.concatenate([high, low], axis=1)
    top = None if first else jnp.max(top_in[0], axis=1, keepdims=True)
    acc = None if first else acc_in[0]
    for j in range(count):
        span = slice(j * rows, (j + 1) * rows)
        s = lax.dot_general(
            pair, kk[span, :], (((1,), (1,)), ((), ())), preferred_element_type=f32
        )
        block_top = jnp.max(s, axis=1, keepdims=True)
        new_top = block_top if top is None else jnp.maximum(top, block_top)
        raised = jnp.exp2(s - new_top).astype(bf16)
        part = dot(raised, vv[span, :])
        acc = part if top is None else acc * jnp.exp2(top - new_top) + part
        top = new_top
    if not last:
        out_a[0] = acc
        out_b[0] = jnp.broadcast_to(top, (top.shape[0], HEAD))
        return
    total = acc[:, HEAD:]
    normal = acc[:, :HEAD] / total
    level = top + jnp.log2(total)
    first_core = where_ref[0] == 0
    lane = lax.broadcasted_iota(jnp.int32, (64, HEAD), 1)
    for z in range(BQ // 128):
        a = slice(z * 128, z * 128 + 64)
        b = slice(z * 128 + 64, z * 128 + 128)
        out_a[0, z, :, :HEAD] = jnp.where(first_core, normal[a], normal[b])
        out_a[0, z, :, HEAD:] = jnp.where(first_core, level[a], level[b])
        out_b[0, z, :, :HEAD] = jnp.where(first_core, normal[b], normal[a]).astype(bf16)
        sent = jnp.where(first_core, level[b], level[a])
        l0 = sent.astype(bf16).astype(f32)
        l1 = (sent - l0).astype(bf16).astype(f32)
        l2 = sent - l0 - l1
        out_b[0, z, :, HEAD:] = jnp.where(lane < 32, l0, jnp.where(lane < 64, l1, l2)).astype(bf16)


def attend(where, own, sib, kvs, state, last):
    tokens = own.shape[0]
    rows = kvs[0].shape[0]
    first = state is None
    count = len(kvs)
    q_spec = pl.BlockSpec((BQ, HEAD), lambda h, i, w: (i, 0))
    kv_spec = pl.BlockSpec((rows, 2 * HEAD), lambda h, i, w: (0, 0))
    acc_spec = pl.BlockSpec((1, BQ, 2 * HEAD), lambda h, i, w: (h, i, 0))
    top_spec = pl.BlockSpec((1, BQ, HEAD), lambda h, i, w: (h, i, 0))
    if last:
        out_spec = pl.BlockSpec((1, BQ // 128, 64, 2 * HEAD), lambda h, i, w: (h, i, 0, 0))
        out_specs = [out_spec, out_spec]
        out_shape = [
            jax.ShapeDtypeStruct((2, tokens // 128, 64, 2 * HEAD), f32),
            jax.ShapeDtypeStruct((2, tokens // 128, 64, 2 * HEAD), bf16),
        ]
    else:
        out_specs = [acc_spec, top_spec]
        out_shape = [
            jax.ShapeDtypeStruct((2, tokens, 2 * HEAD), f32),
            jax.ShapeDtypeStruct((2, tokens, HEAD), f32),
        ]
    return pl.pallas_call(
        functools.partial(attend_kernel, first, last, count),
        grid_spec=pltpu.PrefetchScalarGridSpec(
            num_scalar_prefetch=1,
            grid=(2, tokens // BQ),
            in_specs=[q_spec, q_spec]
            + [kv_spec] * count
            + ([] if first else [acc_spec, top_spec]),
            out_specs=out_specs,
            scratch_shapes=[
                pltpu.VMEM((count * rows, 2 * HEAD), bf16),
                pltpu.VMEM((count * rows, 2 * HEAD), bf16),
            ],
        ),
        out_shape=out_shape,
        compiler_params=room(28),
        name="attend",
    )(where, own, sib, *kvs, *([] if first else state))


def merge_kernel(where_ref, keep_ref, got_ref, out_ref):
    def merged(mine, other):
        other = other.astype(f32)
        theirs = other[:, HEAD : HEAD + 1] + other[:, HEAD + 32 : HEAD + 33]
        theirs = theirs + other[:, HEAD + 64 : HEAD + 65]
        level = jnp.maximum(mine[:, HEAD:], theirs)
        a = jnp.exp2(mine[:, HEAD:] - level)
        b = jnp.exp2(theirs - level)
        return (mine[:, :HEAD] * a + other[:, :HEAD] * b) / (a + b)

    first_core = where_ref[0] == 0
    for z in range(keep_ref.shape[1]):
        own = merged(keep_ref[0, z], got_ref[1, z])
        sib = merged(keep_ref[1, z], got_ref[0, z])
        out_ref[z, :, :HEAD] = jnp.where(first_core, own, sib).astype(bf16)
        out_ref[z, :, HEAD:] = jnp.where(first_core, sib, own).astype(bf16)


def merge(where, keep, got):
    _, z, rows, _ = keep.shape
    return pl.pallas_call(
        merge_kernel,
        grid_spec=pltpu.PrefetchScalarGridSpec(
            num_scalar_prefetch=1,
            grid=(1,),
            in_specs=[pl.BlockSpec(keep.shape, lambda i, w: (0, 0, 0, 0))] * 2,
            out_specs=pl.BlockSpec((z, rows, 2 * HEAD), lambda i, w: (0, 0, 0)),
        ),
        out_shape=jax.ShapeDtypeStruct((z, rows, 2 * HEAD), bf16),
        compiler_params=room(8),
        name="merge",
    )(where, keep, got)


def swap_matrix(experts, blocks):
    count = experts * blocks * 2
    row = lax.broadcasted_iota(jnp.int32, (count, count), 0)
    col = lax.broadcasted_iota(jnp.int32, (count, count), 1)
    a, b, j = row // (blocks * 2), (row // 2) % blocks, row % 2
    return jnp.where(col == b * (experts * 2) + a * 2 + j, 1.0, 0.0).astype(bf16)


def pack(rows_of, out_ref, swap):
    peers = out_ref.shape[0]
    blocks = 16
    tails = []
    for k in range(blocks):
        block = rows_of(k)
        head = block[: peers * 8].reshape(peers, 8, HEAD)
        out_ref[:, k * 8 : (k + 1) * 8, :] = head.astype(bf16)
        tails.append(block[peers * 8 :])
    tail = jnp.concatenate(tails, axis=0).astype(bf16)
    turned = dot(swap, tail)
    out_ref[:, blocks * 8 :, :] = turned.reshape(peers, blocks * 2, HEAD).astype(bf16)


def unpack(in_ref, store, swap):
    peers = in_ref.shape[0]
    blocks = 16
    tail = in_ref[:, blocks * 8 :, :].astype(f32).reshape(peers * blocks * 2, HEAD).astype(bf16)
    turned = dot(swap, tail)
    for k in range(blocks):
        head = in_ref[:, k * 8 : (k + 1) * 8, :].astype(f32).reshape(peers * 8, HEAD)
        store(k, jnp.concatenate([head, turned[k * peers * 2 : (k + 1) * peers * 2]], axis=0))


def slot_of(expert, ordinal, experts):
    return jnp.where(ordinal < 8, expert * 8 + ordinal, experts * 8 + expert * 2 + ordinal - 8)


def project_kernel(
    a_ref, w_ref, res_ref, gain_ref, route_ref, route_t_ref, swap_ref, upd_ref, out_ref, held, sems
):
    steps, rows, depth = a_ref.shape
    copies = [
        pltpu.make_async_copy(
            w_ref.at[pl.ds(i * depth, depth)], held.at[pl.ds(i * depth, depth)], sems.at[i]
        )
        for i in range(steps)
    ]
    for copy in copies:
        copy.start()
    experts = out_ref.shape[0]
    earlier = lax.broadcasted_iota(jnp.int32, (rows, rows), 0)
    later = lax.broadcasted_iota(jnp.int32, (rows, rows), 1)
    slots = lax.broadcasted_iota(jnp.int32, (experts * 10, rows), 0)
    placing = jnp.zeros((experts * 10, rows), f32)
    for t in range(2):
        mine = route_t_ref[t : t + 1, :]
        ordinal = jnp.zeros((1, rows), jnp.int32)
        for u in range(2):
            before = (earlier < later) if u >= t else (earlier <= later)
            same = route_ref[:, u : u + 1] == mine
            ordinal += jnp.sum(jnp.where(before & same, 1, 0), axis=0, keepdims=True)
        placing += jnp.where(slots == slot_of(mine, ordinal, experts), 1.0, 0.0)
    acc = res_ref[...].astype(f32)
    for i in range(steps):
        copies[i].wait()
        acc += dot(a_ref[i], held[i * depth : (i + 1) * depth, :])
    updated = acc.astype(bf16)
    upd_ref[...] = updated
    wide = updated.astype(f32)
    mean = jnp.mean(wide * wide, axis=1, keepdims=True)
    normed = (wide * lax.rsqrt(mean + norm_eps) * gain_ref[...]).astype(bf16)
    sent = dot(placing.astype(bf16), normed)
    pack(lambda k: sent[:, k * HEAD : (k + 1) * HEAD], out_ref, swap_ref[...])


VMEM = pl.BlockSpec(memory_space=pltpu.VMEM)
HBM = pl.BlockSpec(memory_space=pltpu.HBM)


def project(attended, out_weight, residual, norm_gain, route, route_t, swap, peers):
    steps, rows, _ = attended.shape
    width = out_weight.shape[1]
    return pl.pallas_call(
        project_kernel,
        in_specs=[VMEM, HBM, VMEM, VMEM, VMEM, VMEM, VMEM],
        out_specs=[VMEM, VMEM],
        out_shape=[
            jax.ShapeDtypeStruct((rows, width), bf16),
            jax.ShapeDtypeStruct((peers, 160, HEAD), bf16),
        ],
        scratch_shapes=[
            pltpu.VMEM(out_weight.shape, bf16),
            pltpu.SemaphoreType.DMA((steps,)),
        ],
        compiler_params=room(56),
        name="project",
    )(attended, out_weight, residual, norm_gain, route, route_t, swap)


def rows_kernel(in_ref, swap_ref, x_ref):
    def store(k, block):
        x_ref[:, k * HEAD : (k + 1) * HEAD] = block.astype(bf16)

    unpack(in_ref, store, swap_ref[...])


def rows_in(arrived, swap):
    peers = arrived.shape[0]
    return pl.pallas_call(
        rows_kernel,
        in_specs=[VMEM, VMEM],
        out_specs=VMEM,
        out_shape=jax.ShapeDtypeStruct((peers * 10, 16 * HEAD), bf16),
        compiler_params=room(8),
        name="rows_in",
    )(arrived, swap)


def expert_kernel(counts, more, last, own_ref, sib_ref, *refs):
    pieces = []
    for count in counts:
        pieces.append(refs[:count])
        refs = refs[count:]
    if more:
        acc_ref, refs = refs[0], refs[1:]
    out_refs, (x, total) = refs[:-2], refs[-2:]
    rows = own_ref.shape[0]
    width = own_ref.shape[1]

    def take(piece, at, length):
        found, base = [], 0
        for ref in piece:
            lo, hi = max(at - base, 0), min(at + length - base, ref.shape[0])
            if lo < hi:
                found.append(ref[lo:hi, :])
            base += ref.shape[0]
        return found[0] if len(found) == 1 else jnp.concatenate(found, axis=0)

    x[:rows, :] = own_ref[...]
    x[rows:, :] = sib_ref[...]
    parts = []
    for i in range(0, len(pieces), 2):
        pair = pieces[i : i + 2]
        gate = dot(x[...], jnp.concatenate([take(p, 0, width) for p in pair], axis=1))
        up = dot(x[...], jnp.concatenate([take(p, width, width) for p in pair], axis=1))
        parts.append((gate / (1.0 + jnp.exp(-gate)) * up).astype(bf16))
    hid = jnp.concatenate(parts, axis=1)
    for k in range(0, width // HEAD, 2):
        down = jnp.concatenate(
            [
                jnp.concatenate([take(p, 2 * width + c * HEAD, HEAD) for p in pieces], axis=0)
                for c in (k, k + 1)
            ],
            axis=1,
        )
        cols = slice(k * HEAD, (k + 2) * HEAD)
        total[...] = dot(hid, down)
        if more:
            total[...] += acc_ref[:, cols]
        if last:
            keep_ref, send_ref = out_refs
            keep_ref[:, cols] = total[:rows, :]
            send_ref[:, cols] = total[rows:, :].astype(bf16)
        else:
            out_refs[0][:, cols] = total[...]


def expert(own, sib, pieces, acc, last):
    rows, width = own.shape
    flat = [array for piece in pieces for array in piece]
    if last:
        out_shape = [
            jax.ShapeDtypeStruct((rows, width), f32),
            jax.ShapeDtypeStruct((rows, width), bf16),
        ]
    else:
        out_shape = [jax.ShapeDtypeStruct((2 * rows, width), f32)]
    more = [] if acc is None else [acc]
    return pl.pallas_call(
        functools.partial(
            expert_kernel, tuple(len(piece) for piece in pieces), acc is not None, last
        ),
        in_specs=[VMEM] * (2 + len(flat) + len(more)),
        out_specs=[VMEM] * len(out_shape),
        out_shape=out_shape,
        scratch_shapes=[
            pltpu.VMEM((2 * rows, width), bf16),
            pltpu.VMEM((2 * rows, 2 * HEAD), f32),
        ],
        compiler_params=room(40),
        name="expert",
    )(own, sib, *flat, *more)


def finish_kernel(keep_ref, got_ref, swap_ref, out_ref):
    def rows_of(k):
        cols = slice(k * HEAD, (k + 1) * HEAD)
        return keep_ref[:, cols] + got_ref[:, cols].astype(f32)

    pack(rows_of, out_ref, swap_ref[...])


def finish(keep, got, swap, peers):
    return pl.pallas_call(
        finish_kernel,
        in_specs=[VMEM] * 3,
        out_specs=VMEM,
        out_shape=jax.ShapeDtypeStruct((peers, 160, HEAD), bf16),
        compiler_params=room(12),
        name="finish",
    )(keep, got, swap)


def plan_kernel(route_ref, route_t_ref, score_ref, prob_ref, pick_ref, mix_ref, swap_ref):
    rows = route_ref.shape[0]
    experts = pick_ref.shape[2] // 10
    later = lax.broadcasted_iota(jnp.int32, (rows, rows), 0)
    earlier = lax.broadcasted_iota(jnp.int32, (rows, rows), 1)
    slots = lax.broadcasted_iota(jnp.int32, (rows, experts * 10), 1)
    scores = score_ref[...]
    raised = jnp.exp(scores - jnp.max(scores, axis=1, keepdims=True))
    mixing = prob_ref[...] * (raised / jnp.sum(raised, axis=1, keepdims=True))
    for t in range(2):
        mine = route_ref[:, t : t + 1]
        ordinal = jnp.zeros((rows, 1), jnp.int32)
        for u in range(2):
            before = (earlier < later) if u >= t else (earlier <= later)
            same = route_t_ref[u : u + 1, :] == mine
            ordinal += jnp.sum(jnp.where(before & same, 1, 0), axis=1, keepdims=True)
        placed = slots == slot_of(mine, ordinal, experts)
        pick_ref[t] = jnp.where(placed, 1.0, 0.0).astype(bf16)
        mix_ref[t] = jnp.broadcast_to(mixing[:, t : t + 1], (rows, HEAD))
    swap_ref[...] = swap_matrix(experts, 16)


def plan(route, route_t, scores, prob, experts):
    rows = route.shape[0]
    return pl.pallas_call(
        plan_kernel,
        in_specs=[VMEM] * 4,
        out_specs=[VMEM] * 3,
        out_shape=[
            jax.ShapeDtypeStruct((2, rows, experts * 10), bf16),
            jax.ShapeDtypeStruct((2, rows, HEAD), f32),
            jax.ShapeDtypeStruct((experts * 32, experts * 32), bf16),
        ],
        compiler_params=room(8),
        name="plan",
    )(route, route_t, scores, prob)


def mix_kernel(in_ref, upd_ref, pick_ref, mix_ref, swap_ref, out_ref):
    def store(k, block):
        block = block.astype(bf16)
        cols = slice(k * HEAD, (k + 1) * HEAD)
        combined = sum(dot(pick_ref[t], block) * mix_ref[t] for t in range(2))
        out_ref[:, cols] = (upd_ref[:, cols].astype(f32) + combined).astype(bf16)

    unpack(in_ref, store, swap_ref[...])


def mix(returned, updated, picks, mixing, swap):
    return pl.pallas_call(
        mix_kernel,
        in_specs=[VMEM] * 5,
        out_specs=VMEM,
        out_shape=jax.ShapeDtypeStruct(updated.shape, bf16),
        compiler_params=room(12),
        name="mix",
    )(returned, updated, picks, mixing, swap)


def shift(value, axis, by):
    size = lax.axis_size(axis)
    return lax.ppermute(value, axis, [(i, (i + by) % size) for i in range(size)])


def onward(value, axis):
    size = lax.axis_size(axis)
    pairs = []
    for i in range(size):
        pairs.append((2 * i, 2 * ((i + 1) % size)))
        pairs.append((2 * i + 1, 2 * ((i - 1) % size) + 1))
    return lax.ppermute(value, (axis, "core"), pairs)


def swap_cores(value):
    return lax.ppermute(value, "core", ((0, 1), (1, 0)))


def local(
    queries,
    keys,
    values,
    query_gain,
    key_gain,
    out_weight,
    residual,
    norm_gain,
    route_experts,
    expert_scores,
    group_prob,
    w_gate,
    w_up,
    w_down,
):
    peers = lax.axis_size(SP)
    core = lax.axis_index("core")
    z = lax.axis_index("z")
    seq = lax.axis_index(SP)
    tokens = queries.shape[0]

    where = jnp.stack([core, z // 2]).astype(jnp.int32)
    lane = jnp.arange(HEAD, dtype=jnp.int32)
    pair = (lane // 2) % (HEAD // 4)
    frequency = rope_base ** (-pair.astype(f32) * 4.0 / HEAD)
    grid_rows = tokens // GRID_W
    place = jnp.arange(grid_rows + GRID_W, dtype=jnp.int32)
    place = jnp.where(place < grid_rows, seq * grid_rows + place, place - grid_rows)
    angles = place.astype(f32)[:, None] * frequency[None, :]
    cosine = jnp.cos(angles)
    sine = jnp.sin(angles) * jnp.where(lane % 2 == 0, -1.0, 1.0)[None, :]

    w0 = bundle(w_gate[0], w_up[0], w_down[0]).reshape(-1, HEAD)
    w1p, w1m = shift(w0, "z", 1), shift(w0, "z", -1)
    route_t = route_experts.T
    picks, mixing, swap = plan(
        route_experts, route_t, expert_scores, group_prob[:, None], peers
    )
    own, kv_a, kv_b = prep(
        where, queries, keys, values, query_gain[None, :], key_gain[None, :], cosine, sine
    )
    ax = jnp.concatenate([kv_a] + [shift(kv_a, "x", d) for d in (1, -1, 2)], axis=0)
    by = jnp.concatenate([kv_b] + [shift(kv_b, "y", d) for d in (1, -1, 2)], axis=0)
    sib = swap_cores(own)
    a_next = [shift(ax, "y", 1), shift(ax, "y", -1)]
    b_next = [shift(by, "x", 1), shift(by, "x", -1)]
    state = attend(where, own, sib, [ax, by], None, False)
    w1p, w1m, state, a_next, b_next = lax.optimization_barrier((w1p, w1m, state, a_next, b_next))
    w2p, w2m = shift(w1p, "z", 1), shift(w1m, "z", -1)
    a_far = onward(jnp.where(core == 0, a_next[0], a_next[1]), "y")
    b_far = onward(jnp.where(core == 0, b_next[0], b_next[1]), "x")
    state = attend(where, own, sib, a_next + b_next, state, False)
    keep, send = attend(where, own, sib, [a_far, b_far], state, True)
    got = swap_cores(send)
    w2p, w2m, _ = lax.optimization_barrier((w2p, w2m, keep))
    third = w0.shape[0] // 3
    w3p = [shift(w2p[:third], "z", 1)]
    w3m = [shift(w2m[:third], "z", -1)]
    merged = merge(where, keep, got)
    attended = lax.all_to_all(merged, "z", 0, 0, tiled=True)
    rest_p, rest_m, attended = lax.optimization_barrier((w2p[third:], w2m[third:], attended))
    w3p.append(shift(rest_p, "z", 1))
    w3m.append(shift(rest_m, "z", -1))
    updated, outgoing = project(
        attended, out_weight, residual, norm_gain[None, :], route_experts, route_t, swap, peers
    )
    arrived = lax.all_to_all(outgoing, SP, 0, 0, tiled=True)
    w3p, w3m, arrived = lax.optimization_barrier((w3p, w3m, arrived))
    w4 = [
        shift(w3p[0], "z", 1),
        shift(w3p[1][: third // 2], "z", 1),
        shift(w3m[1][third // 2 :], "z", -1),
    ]
    rows = rows_in(arrived, swap)
    sib_rows = swap_cores(rows)
    (acc,) = expert(rows, sib_rows, [[w0], [w1p], [w1m], [w2p], [w2m], w3p], None, False)
    keep, send = expert(rows, sib_rows, [w3m, w4], acc, True)
    result = finish(keep, swap_cores(send), swap, peers)
    returned = lax.all_to_all(result, SP, 0, 0, tiled=True)
    return mix(returned, updated, picks, mixing, swap)


def solution(mesh):
    torus = Mesh(mesh.devices.reshape(4, 4, 8, 2), ("y", "x", "z", "core"))
    placed = (
        P(SP, TP),
        P(SP, None),
        P(SP, None),
        P(TP),
        P(),
        P(),
        P(SP_TP, None),
        P(),
        P(SP_TP, None),
        P(SP_TP, None),
        P(SP_TP),
        P(SP, None, TP),
        P(SP, None, TP),
        P(SP, TP, None),
    )
    return jax.shard_map(
        local, mesh=torus, in_specs=placed, out_specs=P(SP_TP, None), check_vma=False
    )
```

profile of v0, /device:TPU:1, one launch (start us, length us, event | category | flops | bytes accessed | tf_op | source)
XLA Modules:
  0.0 206.3 jit_solution(11141111169128189695)
XLA Ops:
  0.0 2.4 %bundle.1 = bf16[3,2048,128]{2,1,0:T(8,128)(2,1)} custom-call(bf16[2048,128]{1,0:T(8,128)(2,1)} %bitcast.16, bf16[2048,128]{1,0:T(8,128)(2,1)} %bitcast.17, bf16[128,2048]{1,0:T(8,128)(2,1)} %bitcast.18), custom_call_target="tpu_custom_call" | custom-call | tf_op jit(solution)/shard_map/bundle/pallas_call | solution.py:43
  2.4 2.5 %collective-permute-start = (bf16[6144,128]{1,0:T(8,128)(2,1)}, bf16[6144,128]{1,0:T(8,128)(2,1)}, u32[]{:S(2)}, u32[]{:S(2)}) collective-permute-start(bf16[6144,128]{1,0:T(8,128)(2,1)} %bitcast.11), channel_id=1, source_target_pairs={{0,2},{2,4},{4,6},{6,8},{8,10},{10,12},{12,14},{14,0},{1,3},{3,5},... | collective-permute-start | bytes 4718600 | tf_op jit(solution)/shard_map/ppermute | solution.py:533
  4.8 3.9 %collective-permute-start.1 = (bf16[6144,128]{1,0:T(8,128)(2,1)}, bf16[6144,128]{1,0:T(8,128)(2,1)}, u32[]{:S(2)}, u32[]{:S(2)}) collective-permute-start(bf16[6144,128]{1,0:T(8,128)(2,1)} %bitcast.12), channel_id=1, source_target_pairs={{0,14},{2,0},{4,2},{6,4},{8,6},{10,8},{12,10},{14,12},{1,15},{3,1}... | collective-permute-start | bytes 4718600 | tf_op jit(solution)/shard_map/ppermute | solution.py:533
  8.8 0.9 fusion
  9.7 0.6 pad_add_fusion.where_ref
  10.3 5.2 %prep.1 = (bf16[1024,128]{1,0:T(8,128)(2,1)}, bf16[256,256]{1,0:T(8,128)(2,1)}, bf16[256,256]{1,0:T(8,128)(2,1)}) custom-call(s32[2]{0:T(128)} %pad_add_fusion.where_ref, bf16[1024,128]{1,0:T(8,128)(2,1)} %q_ref.1, bf16[1024,512]{1,0:T(8,128)(2,1)} %k_ref.1, bf16[1024,512]{1,0:T(8,128)(2,1)} %v_ref.1, f32[1,128]{1,0:T(1,128)} %bitcast.20, ...), custom_call_target="tpu_custom_call" | custom-call | tf_op jit(solution)/shard_map/prep/pallas_call | solution.py:95
  15.4 1.2 collective-permute-start.3
  16.6 1.5 collective-permute-start.4
  18.1 1.5 collective-permute-start.5
  19.6 0.9 constant_dynamic-update-slice_fusion.3
  20.6 0.5 collective-permute-done.3
  21.1 3.9 %collective-permute-done.5 = bf16[256,256]{1,0:T(8,128)(2,1)S(1)} collective-permute-done((bf16[256,256]{1,0:T(8,128)(2,1)}, bf16[256,256]{1,0:T(8,128)(2,1)S(1)}, u32[]{:S(2)}, u32[]{:S(2)}) %collective-permute-start.5) | collective-permute-done | bytes 131104 | tf_op jit(solution)/shard_map/ppermute | solution.py:533
  25.0 2.8 %collective-permute-start.10 = (bf16[1024,256]{1,0:T(8,128)(2,1)S(1)}, bf16[1024,256]{1,0:T(8,128)(2,1)S(1)}, u32[]{:S(2)}, u32[]{:S(2)}) collective-permute-start(bf16[1024,256]{1,0:T(8,128)(2,1)S(1)} %constant_dynamic-update-slice_fusion.refs_0_), channel_id=1, source_target_pairs={{0,192},{64,0},{128,64},{192,128},{1,193},{65,1},{129,65},{193,129... | collective-permute-start | bytes 1572872 | tf_op jit(solution)/shard_map/ppermute | solution.py:533
  27.8 2.7 %collective-permute-start.7 = (bf16[256,256]{1,0:T(8,128)(2,1)}, bf16[256,256]{1,0:T(8,128)(2,1)S(1)}, u32[]{:S(2)}, u32[]{:S(2)}) collective-permute-start(bf16[256,256]{1,0:T(8,128)(2,1)} %get-tuple-element.41), channel_id=1, source_target_pairs={{0,192},{64,0},{128,64},{192,128},{1,193},{65,1},{129,65},{193,129... | collective-permute-start | bytes 393224 | tf_op jit(solution)/shard_map/ppermute | solution.py:533
  30.5 0.9 constant_dynamic-update-slice_fusion.7
  31.5 2.0 collective-permute-done.6
  33.5 8.1 %collective-permute-done.7 = bf16[256,256]{1,0:T(8,128)(2,1)S(1)} collective-permute-done((bf16[256,256]{1,0:T(8,128)(2,1)}, bf16[256,256]{1,0:T(8,128)(2,1)S(1)}, u32[]{:S(2)}, u32[]{:S(2)}) %collective-permute-start.7) | collective-permute-done | bytes 131104 | tf_op jit(solution)/shard_map/ppermute | solution.py:533
  41.5 4.2 %collective-permute-start.2 = (bf16[1024,128]{1,0:T(8,128)(2,1)}, bf16[1024,128]{1,0:T(8,128)(2,1)S(1)}, u32[]{:S(2)}, u32[]{:S(2)}) collective-permute-start(bf16[1024,128]{1,0:T(8,128)(2,1)} %get-tuple-element.39.own_ref), channel_id=1, source_target_pairs={{0,1},{1,0},{2,3},{3,2},{4,5},{5,4},{6,7},{7,6},{8,9},{9,8},{10,11... | collective-permute-start | bytes 786440 | tf_op jit(solution)/shard_map/ppermute | solution.py:546
  45.8 0.5 collective-permute-start.11
  46.2 0.8 collective-permute-done.2.sib_ref
  47.1 1.6 collective-permute-start.12
  48.7 10.1 %attend.3 = (f32[2,1024,256]{2,1,0:T(8,128)S(1)}, f32[2,1024,128]{2,1,0:T(8,128)S(1)}) custom-call(s32[2]{0:T(128)S(1)} %copy-done.10, bf16[1024,128]{1,0:T(8,128)(2,1)S(1)} %copy-done.3, bf16[1024,128]{1,0:T(8,128)(2,1)S(1)} %collective-permute-done.2.sib_ref, bf16[1024,256]{1,0:T(8,128)(2,1)S(1)} %constant_dynamic-update-slice_fusion.refs_0_, ...), custom_call_target="tpu_custom_call" | custom-call | tf_op jit(solution)/shard_map/attend/pallas_call | solution.py:206
  58.8 1.8 collective-permute-done.11.refs_2_
  60.6 3.1 %collective-permute-done.9.refs_0_ = bf16[1024,256]{1,0:T(8,128)(2,1)} collective-permute-done((bf16[1024,256]{1,0:T(8,128)(2,1)S(1)}, bf16[1024,256]{1,0:T(8,128)(2,1)}, u32[]{:S(2)}, u32[]{:S(2)}) %collective-permute-start.9) | collective-permute-done | bytes 524320 | tf_op jit(solution)/shard_map/ppermute | solution.py:533
  63.8 0.4 collective-permute-start.16
  64.2 2.7 %collective-permute-start.14 = (bf16[6144,128]{1,0:T(8,128)(2,1)}, bf16[6144,128]{1,0:T(8,128)(2,1)}, u32[]{:S(2)}, u32[]{:S(2)}) collective-permute-start(bf16[6144,128]{1,0:T(8,128)(2,1)} %collective-permute-done.1.refs_2_), channel_id=1, source_target_pairs={{0,14},{2,0},{4,2},{6,4},{8,6},{10,8},{12,10},{14,12},{1,15},{3,1}... | collective-permute-start | bytes 4718600 | tf_op jit(solution)/shard_map/ppermute | solution.py:533
  66.9 0.1 broadcast_select_fusion.1
  67.0 3.0 %collective-permute-start.15 = (bf16[1024,256]{1,0:T(8,128)(2,1)S(1)}, bf16[1024,256]{1,0:T(8,128)(2,1)S(1)}, u32[]{:S(2)}, u32[]{:S(2)}) collective-permute-start(bf16[1024,256]{1,0:T(8,128)(2,1)S(1)} %broadcast_select_fusion.1), channel_id=1, source_target_pairs={{0,64},{1,193},{64,128},{65,1},{128,192},{129,65},{192,0},{193,129... | collective-permute-start | bytes 1572872 | tf_op jit(solution)/shard_map/ppermute | solution.py:542
  69.9 16.2 %attend.4 = (f32[2,1024,256]{2,1,0:T(8,128)S(1)}, f32[2,1024,128]{2,1,0:T(8,128)S(1)}) custom-call(s32[2]{0:T(128)S(1)} %copy-done.10, bf16[1024,128]{1,0:T(8,128)(2,1)S(1)} %copy-done.3, bf16[1024,128]{1,0:T(8,128)(2,1)S(1)} %collective-permute-done.2.sib_ref, bf16[1024,256]{1,0:T(8,128)(2,1)} %collective-permute-done.9.refs_0_, ...), custom_call_target="tpu_custom_call" | custom-call | tf_op jit(solution)/shard_map/attend/pallas_call | solution.py:206
  86.1 10.4 %attend.5 = (f32[2,8,64,256]{3,2,1,0:T(8,128)S(1)}, bf16[2,8,64,256]{3,2,1,0:T(8,128)(2,1)S(1)}) custom-call(s32[2]{0:T(128)S(1)} %copy-done.10, bf16[1024,128]{1,0:T(8,128)(2,1)S(1)} %copy-done.3, bf16[1024,128]{1,0:T(8,128)(2,1)S(1)} %collective-permute-done.2.sib_ref, bf16[1024,256]{1,0:T(8,128)(2,1)S(1)} %collective-permute-done.15.refs_0_, ...), custom_call_target="tpu_custom_call" | custom-call | tf_op jit(solution)/shard_map/attend/pallas_call | solution.py:206
  96.5 0.1 collective-permute-start.18
  96.6 1.9 collective-permute-done.18.got_ref
  98.5 2.3 %merge.1 = bf16[8,64,256]{2,1,0:T(8,128)(2,1)} custom-call(s32[2]{0:T(128)S(1)} %copy-done.10, f32[2,8,64,256]{3,2,1,0:T(8,128)S(1)} %get-tuple-element.54.keep_ref, bf16[2,8,64,256]{3,2,1,0:T(8,128)(2,1)S(1)} %collective-permute-done.18.got_ref), custom_call_target="tpu_custom_call" | custom-call | tf_op jit(solution)/shard_map/merge/pallas_call | solution.py:246
  100.8 5.5 %all-to-all-start = ((bf16[8,64,256]{2,1,0:T(8,128)(2,1)}), bf16[8,64,256]{2,1,0:T(8,128)(2,1)S(1)}, u32[]{:S(2)}, u32[]{:S(2)}) async-start(bf16[8,64,256]{2,1,0:T(8,128)(2,1)} %merge.1), calls=%async_computation | async-start | bytes 524288 | tf_op jit(solution)/shard_map/all_to_all | solution.py:609
  106.3 1.0 slice.19
  107.4 2.4 %slice.20 = bf16[4096,128]{1,0:T(8,128)(2,1)} slice(bf16[6144,128]{1,0:T(8,128)(2,1)} %collective-permute-done.14.refs_4_), slice={[2048:6144], [0:128]} | slice | bytes 2097152 | tf_op jit(solution)/shard_map/slice | solution.py:610
  109.8 8.8 %all-to-all-done.a_ref = bf16[8,64,256]{2,1,0:T(8,128)(2,1)S(1)} async-done(((bf16[8,64,256]{2,1,0:T(8,128)(2,1)}), bf16[8,64,256]{2,1,0:T(8,128)(2,1)S(1)}, u32[]{:S(2)}, u32[]{:S(2)}) %all-to-all-start) | async-done | bytes 262176 | tf_op jit(solution)/shard_map/all_to_all | solution.py:609
  118.6 2.7 %collective-permute-start.21 = (bf16[4096,128]{1,0:T(8,128)(2,1)}, bf16[4096,128]{1,0:T(8,128)(2,1)S(1)}, u32[]{:S(2)}, u32[]{:S(2)}) collective-permute-start(bf16[4096,128]{1,0:T(8,128)(2,1)} %slice.20), channel_id=1, source_target_pairs={{0,14},{2,0},{4,2},{6,4},{8,6},{10,8},{12,10},{14,12},{1,15},{3,1}... | collective-permute-start | bytes 3145736 | tf_op jit(solution)/shard_map/ppermute | solution.py:533
  121.3 0.1 copy.18.route_ref
  121.4 0.1 copy.16.score_ref
  121.5 0.1 copy.17.prob_ref
  121.6 0.7 plan.1
  122.3 0.8 copy-done
  123.2 6.6 %project.1 = (bf16[64,2048]{1,0:T(8,128)(2,1)}, bf16[16,160,128]{2,1,0:T(8,128)(2,1)}) custom-call(bf16[8,64,256]{2,1,0:T(8,128)(2,1)} %copy-done.12, bf16[2048,2048]{1,0:T(8,128)(2,1)} %w_ref.1, bf16[64,2048]{1,0:T(8,128)(2,1)} %res_ref.1, f32[1,2048]{1,0:T(1,128)} %bitcast.19, s32[64,2]{1,0:T(8,128)} %copy-done.8, s32[2,64]{1,0:T(2,128)} %bitcast.14, ...), custom_call_target="tpu_custom_call" | custom-call | tf_op jit(solution)/shard_map/project/pallas_call | solution.py:341
  129.7 5.3 %all-to-all-start.1 = ((bf16[16,160,128]{2,1,0:T(8,128)(2,1)}), bf16[16,160,128]{2,1,0:T(8,128)(2,1)}, u32[]{:S(2)}, u32[]{:S(2)}) async-start(bf16[16,160,128]{2,1,0:T(8,128)(2,1)} %get-tuple-element.62), calls=%async_computation.1 | async-start | bytes 1310720 | tf_op jit(solution)/shard_map/all_to_all | solution.py:616
  135.1 1.1 slice.21
  136.2 0.1 collective-permute-start.17
  136.3 2.7 %collective-permute-start.20 = (bf16[2048,128]{1,0:T(8,128)(2,1)S(1)}, bf16[2048,128]{1,0:T(8,128)(2,1)S(1)}, u32[]{:S(2)}, u32[]{:S(2)}) collective-permute-start(bf16[2048,128]{1,0:T(8,128)(2,1)S(1)} %slice.21), channel_id=1, source_target_pairs={{0,14},{2,0},{4,2},{6,4},{8,6},{10,8},{12,10},{14,12},{1,15},{3,1}... | collective-permute-start | bytes 1572872 | tf_op jit(solution)/shard_map/ppermute | solution.py:533
  139.0 16.6 %collective-permute-done.17.refs_5_ = bf16[2048,128]{1,0:T(8,128)(2,1)} collective-permute-done((bf16[2048,128]{1,0:T(8,128)(2,1)S(1)}, bf16[2048,128]{1,0:T(8,128)(2,1)}, u32[]{:S(2)}, u32[]{:S(2)}) %collective-permute-start.17) | collective-permute-done | bytes 524320 | tf_op jit(solution)/shard_map/ppermute | solution.py:533
  155.5 0.8 copy-done.6
  156.4 2.4 %collective-permute-start.25 = (bf16[3072,128]{1,0:T(8,128)(2,1)S(1)}, bf16[3072,128]{1,0:T(8,128)(2,1)S(1)}, u32[]{:S(2)}, u32[]{:S(2)}) collective-permute-start(bf16[3072,128]{1,0:T(8,128)(2,1)S(1)} %slice.23), channel_id=1, source_target_pairs={{0,14},{2,0},{4,2},{6,4},{8,6},{10,8},{12,10},{14,12},{1,15},{3,1}... | collective-permute-start | bytes 2359304 | tf_op jit(solution)/shard_map/ppermute | solution.py:533
  158.7 1.5 rows_in.1.own_ref
  160.3 2.1 %collective-permute-start.22 = (bf16[160,2048]{1,0:T(8,128)(2,1)S(1)}, bf16[160,2048]{1,0:T(8,128)(2,1)S(1)}, u32[]{:S(2)}, u32[]{:S(2)}) collective-permute-start(bf16[160,2048]{1,0:T(8,128)(2,1)S(1)} %rows_in.1.own_ref), channel_id=1, source_target_pairs={{0,1},{1,0},{2,3},{3,2},{4,5},{5,4},{6,7},{7,6},{8,9},{9,8},{10,11... | collective-permute-start | bytes 1966088 | tf_op jit(solution)/shard_map/ppermute | solution.py:546
  162.3 1.0 slice.22
  163.3 0.1 collective-permute-start.24
  163.4 0.6 collective-permute-done.22.sib_ref
  164.1 6.0 %expert.2.refs_5_ = f32[320,2048]{1,0:T(8,128)S(1)} custom-call(bf16[160,2048]{1,0:T(8,128)(2,1)S(1)} %rows_in.1.own_ref, bf16[160,2048]{1,0:T(8,128)(2,1)S(1)} %collective-permute-done.22.sib_ref, bf16[6144,128]{1,0:T(8,128)(2,1)S(1)} %bitcast.13, bf16[6144,128]{1,0:T(8,128)(2,1)} %collective-permute-done.refs_1_, ...), custom_call_target="tpu_custom_call" | custom-call | tf_op jit(solution)/shard_map/expert/pallas_call | solution.py:437
  170.1 12.7 %collective-permute-done.24.refs_3_ = bf16[1024,128]{1,0:T(8,128)(2,1)S(1)} collective-permute-done((bf16[1024,128]{1,0:T(8,128)(2,1)S(1)}, bf16[1024,128]{1,0:T(8,128)(2,1)S(1)}, u32[]{:S(2)}, u32[]{:S(2)}) %collective-permute-start.24) | collective-permute-done | bytes 262176 | tf_op jit(solution)/shard_map/ppermute | solution.py:533
  182.8 1.3 expert.3
  184.0 1.0 collective-permute-start.26
  185.1 1.7 collective-permute-done.26.got_ref
  186.8 0.4 finish.1
  187.3 17.5 %all_to_all.15.in_ref = bf16[16,160,128]{2,1,0:T(8,128)(2,1)S(1)} all-to-all(bf16[16,160,128]{2,1,0:T(8,128)(2,1)S(1)} %finish.1), channel_id=1, replica_groups=mesh['y'=4,'x'=4,'z'=8,'core'=2] {'y','x'}, dimensions={0} | all-to-all | bytes 1310720 | tf_op jit(solution)/shard_map/all_to_all | solution.py:628
  204.7 1.6 mix.1
  (61 shorter events, 0.3 us)
Async XLA Ops:
  2.4 61.4 %collective-permute-start = (bf16[6144,128]{1,0:T(8,128)(2,1)}, bf16[6144,128]{1,0:T(8,128)(2,1)}, u32[]{:S(2)}, u32[]{:S(2)}) collective-permute-start(bf16[6144,128]{1,0:T(8,128)(2,1)} %bitcast.11), channel_id=1, source_target_pairs={{0,2},{2,4},{4,6},{6,8},{8,10},{10,12},{12,14},{14,0},{1,3},{3,5},... | collective-permute-start | bytes 4718600 | tf_op jit(solution)/shard_map/ppermute | solution.py:533
  4.8 58.9 %collective-permute-start.1 = (bf16[6144,128]{1,0:T(8,128)(2,1)}, bf16[6144,128]{1,0:T(8,128)(2,1)}, u32[]{:S(2)}, u32[]{:S(2)}) collective-permute-start(bf16[6144,128]{1,0:T(8,128)(2,1)} %bitcast.12), channel_id=1, source_target_pairs={{0,14},{2,0},{4,2},{6,4},{8,6},{10,8},{12,10},{14,12},{1,15},{3,1}... | collective-permute-start | bytes 4718600 | tf_op jit(solution)/shard_map/ppermute | solution.py:533
  15.4 33.2 %copy-start.3 = (bf16[1024,128]{1,0:T(8,128)(2,1)S(1)}, bf16[1024,128]{1,0:T(8,128)(2,1)}, u32[]{:S(2)}) copy-start(bf16[1024,128]{1,0:T(8,128)(2,1)} %get-tuple-element.39.own_ref) | copy-start | bytes 786436
  15.4 33.3 %copy-start.10 = (s32[2]{0:T(128)S(1)}, s32[2]{0:T(128)}, u32[]{:S(2)}) copy-start(s32[2]{0:T(128)} %pad_add_fusion.where_ref) | copy-start | bytes 28
  15.4 5.6 %collective-permute-start.3 = (bf16[256,256]{1,0:T(8,128)(2,1)}, bf16[256,256]{1,0:T(8,128)(2,1)S(1)}, u32[]{:S(2)}, u32[]{:S(2)}) collective-permute-start(bf16[256,256]{1,0:T(8,128)(2,1)} %get-tuple-element.40), channel_id=1, source_target_pairs={{0,16},{16,32},{32,48},{48,0},{1,17},{17,33},{33,49},{49,1},{2,18}... | collective-permute-start | bytes 393224 | tf_op jit(solution)/shard_map/ppermute | solution.py:533
  16.6 4.4 %collective-permute-start.4 = (bf16[256,256]{1,0:T(8,128)(2,1)}, bf16[256,256]{1,0:T(8,128)(2,1)S(1)}, u32[]{:S(2)}, u32[]{:S(2)}) collective-permute-start(bf16[256,256]{1,0:T(8,128)(2,1)} %get-tuple-element.40), channel_id=1, source_target_pairs={{0,48},{16,0},{32,16},{48,32},{1,49},{17,1},{33,17},{49,33},{2,50}... | collective-permute-start | bytes 393224 | tf_op jit(solution)/shard_map/ppermute | solution.py:533
  18.1 6.9 %collective-permute-start.5 = (bf16[256,256]{1,0:T(8,128)(2,1)}, bf16[256,256]{1,0:T(8,128)(2,1)S(1)}, u32[]{:S(2)}, u32[]{:S(2)}) collective-permute-start(bf16[256,256]{1,0:T(8,128)(2,1)} %get-tuple-element.40), channel_id=1, source_target_pairs={{0,32},{16,48},{32,0},{48,16},{1,33},{17,49},{33,1},{49,17},{2,34}... | collective-permute-start | bytes 393224 | tf_op jit(solution)/shard_map/ppermute | solution.py:533
  25.0 23.6 %collective-permute-start.10 = (bf16[1024,256]{1,0:T(8,128)(2,1)S(1)}, bf16[1024,256]{1,0:T(8,128)(2,1)S(1)}, u32[]{:S(2)}, u32[]{:S(2)}) collective-permute-start(bf16[1024,256]{1,0:T(8,128)(2,1)S(1)} %constant_dynamic-update-slice_fusion.refs_0_), channel_id=1, source_target_pairs={{0,192},{64,0},{128,64},{192,128},{1,193},{65,1},{129,65},{193,129... | collective-permute-start | bytes 1572872 | tf_op jit(solution)/shard_map/ppermute | solution.py:533
  27.8 5.6 %collective-permute-start.6 = (bf16[256,256]{1,0:T(8,128)(2,1)}, bf16[256,256]{1,0:T(8,128)(2,1)S(1)}, u32[]{:S(2)}, u32[]{:S(2)}) collective-permute-start(bf16[256,256]{1,0:T(8,128)(2,1)} %get-tuple-element.41), channel_id=1, source_target_pairs={{0,64},{64,128},{128,192},{192,0},{1,65},{65,129},{129,193},{193,1... | collective-permute-start | bytes 393224 | tf_op jit(solution)/shard_map/ppermute | solution.py:533
  27.8 13.7 %collective-permute-start.7 = (bf16[256,256]{1,0:T(8,128)(2,1)}, bf16[256,256]{1,0:T(8,128)(2,1)S(1)}, u32[]{:S(2)}, u32[]{:S(2)}) collective-permute-start(bf16[256,256]{1,0:T(8,128)(2,1)} %get-tuple-element.41), channel_id=1, source_target_pairs={{0,192},{64,0},{128,64},{192,128},{1,193},{65,1},{129,65},{193,129... | collective-permute-start | bytes 393224 | tf_op jit(solution)/shard_map/ppermute | solution.py:533
  33.5 12.3 %collective-permute-start.8 = (bf16[256,256]{1,0:T(8,128)(2,1)}, bf16[256,256]{1,0:T(8,128)(2,1)S(1)}, u32[]{:S(2)}, u32[]{:S(2)}) collective-permute-start(bf16[256,256]{1,0:T(8,128)(2,1)} %get-tuple-element.41), channel_id=1, source_target_pairs={{0,128},{64,192},{128,0},{192,64},{1,129},{65,193},{129,1},{193,65... | collective-permute-start | bytes 393224 | tf_op jit(solution)/shard_map/ppermute | solution.py:533
  41.5 5.5 %collective-permute-start.2 = (bf16[1024,128]{1,0:T(8,128)(2,1)}, bf16[1024,128]{1,0:T(8,128)(2,1)S(1)}, u32[]{:S(2)}, u32[]{:S(2)}) collective-permute-start(bf16[1024,128]{1,0:T(8,128)(2,1)} %get-tuple-element.39.own_ref), channel_id=1, source_target_pairs={{0,1},{1,0},{2,3},{3,2},{4,5},{5,4},{6,7},{7,6},{8,9},{9,8},{10,11... | collective-permute-start | bytes 786440 | tf_op jit(solution)/shard_map/ppermute | solution.py:546
  45.8 14.9 %collective-permute-start.11 = (bf16[1024,256]{1,0:T(8,128)(2,1)S(1)}, bf16[1024,256]{1,0:T(8,128)(2,1)S(1)}, u32[]{:S(2)}, u32[]{:S(2)}) collective-permute-start(bf16[1024,256]{1,0:T(8,128)(2,1)S(1)} %constant_dynamic-update-slice_fusion.4.refs_1_), channel_id=1, source_target_pairs={{0,16},{16,32},{32,48},{48,0},{1,17},{17,33},{33,49},{49,1},{2,18}... | collective-permute-start | bytes 1572872 | tf_op jit(solution)/shard_map/ppermute | solution.py:533
  47.1 13.6 %collective-permute-start.12 = (bf16[1024,256]{1,0:T(8,128)(2,1)S(1)}, bf16[1024,256]{1,0:T(8,128)(2,1)S(1)}, u32[]{:S(2)}, u32[]{:S(2)}) collective-permute-start(bf16[1024,256]{1,0:T(8,128)(2,1)S(1)} %constant_dynamic-update-slice_fusion.4.refs_1_), channel_id=1, source_target_pairs={{0,48},{16,0},{32,16},{48,32},{1,49},{17,1},{33,17},{49,33},{2,50}... | collective-permute-start | bytes 1572872 | tf_op jit(solution)/shard_map/ppermute | solution.py:533
  48.7 15.1 %collective-permute-start.9 = (bf16[1024,256]{1,0:T(8,128)(2,1)S(1)}, bf16[1024,256]{1,0:T(8,128)(2,1)}, u32[]{:S(2)}, u32[]{:S(2)}) collective-permute-start(bf16[1024,256]{1,0:T(8,128)(2,1)S(1)} %constant_dynamic-update-slice_fusion.refs_0_), channel_id=1, source_target_pairs={{0,64},{64,128},{128,192},{192,0},{1,65},{65,129},{129,193},{193,1... | collective-permute-start | bytes 1572872 | tf_op jit(solution)/shard_map/ppermute | solution.py:533
  60.6 3.2 %copy-start.4 = (bf16[1024,256]{1,0:T(8,128)(2,1)}, bf16[1024,256]{1,0:T(8,128)(2,1)S(1)}, u32[]{:S(2)}) copy-start(bf16[1024,256]{1,0:T(8,128)(2,1)S(1)} %collective-permute-done.12.refs_3_) | copy-start | bytes 1572868
  63.8 22.3 %collective-permute-start.16 = (bf16[1024,256]{1,0:T(8,128)(2,1)S(1)}, bf16[1024,256]{1,0:T(8,128)(2,1)S(1)}, u32[]{:S(2)}, u32[]{:S(2)}) collective-permute-start(bf16[1024,256]{1,0:T(8,128)(2,1)S(1)} %broadcast_select_fusion), channel_id=1, source_target_pairs={{0,16},{1,49},{16,32},{17,1},{32,48},{33,17},{48,0},{49,33},{2,18}... | collective-permute-start | bytes 1572872 | tf_op jit(solution)/shard_map/ppermute | solution.py:542
  64.2 5.7 %copy-start.5 = (bf16[1024,256]{1,0:T(8,128)(2,1)S(1)}, bf16[1024,256]{1,0:T(8,128)(2,1)}, u32[]{:S(2)}) copy-start(bf16[1024,256]{1,0:T(8,128)(2,1)} %copy-done.4) | copy-start | bytes 1572868
  64.2 42.1 %collective-permute-start.13 = (bf16[6144,128]{1,0:T(8,128)(2,1)}, bf16[6144,128]{1,0:T(8,128)(2,1)S(1)}, u32[]{:S(2)}, u32[]{:S(2)}) collective-permute-start(bf16[6144,128]{1,0:T(8,128)(2,1)} %collective-permute-done.refs_1_), channel_id=1, source_target_pairs={{0,2},{2,4},{4,6},{6,8},{8,10},{10,12},{12,14},{14,0},{1,3},{3,5},... | collective-permute-start | bytes 4718600 | tf_op jit(solution)/shard_map/ppermute | solution.py:533
  64.2 42.1 %collective-permute-start.14 = (bf16[6144,128]{1,0:T(8,128)(2,1)}, bf16[6144,128]{1,0:T(8,128)(2,1)}, u32[]{:S(2)}, u32[]{:S(2)}) collective-permute-start(bf16[6144,128]{1,0:T(8,128)(2,1)} %collective-permute-done.1.refs_2_), channel_id=1, source_target_pairs={{0,14},{2,0},{4,2},{6,4},{8,6},{10,8},{12,10},{14,12},{1,15},{3,1}... | collective-permute-start | bytes 4718600 | tf_op jit(solution)/shard_map/ppermute | solution.py:533
  67.0 19.2 %collective-permute-start.15 = (bf16[1024,256]{1,0:T(8,128)(2,1)S(1)}, bf16[1024,256]{1,0:T(8,128)(2,1)S(1)}, u32[]{:S(2)}, u32[]{:S(2)}) collective-permute-start(bf16[1024,256]{1,0:T(8,128)(2,1)S(1)} %broadcast_select_fusion.1), channel_id=1, source_target_pairs={{0,64},{1,193},{64,128},{65,1},{128,192},{129,65},{192,0},{193,129... | collective-permute-start | bytes 1572872 | tf_op jit(solution)/shard_map/ppermute | solution.py:542
  96.5 2.0 collective-permute-start.18
  100.8 17.8 %all-to-all-start = ((bf16[8,64,256]{2,1,0:T(8,128)(2,1)}), bf16[8,64,256]{2,1,0:T(8,128)(2,1)S(1)}, u32[]{:S(2)}, u32[]{:S(2)}) async-start(bf16[8,64,256]{2,1,0:T(8,128)(2,1)} %merge.1), calls=%async_computation | async-start | bytes 524288 | tf_op jit(solution)/shard_map/all_to_all | solution.py:609
  107.4 13.9 %copy-start.11 = (s32[64,2]{0,1:T(2,128)S(1)}, s32[64,2]{0,1:T(2,128)}, u32[]{:S(2)}) copy-start(s32[64,2]{0,1:T(2,128)} %param.22) | copy-start | bytes 1540
  107.4 14.0 %copy-start.13 = (f32[64,2]{0,1:T(2,128)S(1)}, f32[64,2]{0,1:T(2,128)}, u32[]{:S(2)}) copy-start(f32[64,2]{0,1:T(2,128)} %param.23) | copy-start | bytes 1540
  107.4 14.1 %copy-start.14 = (f32[64]{0:T(128)S(1)}, f32[64]{0:T(128)}, u32[]{:S(2)}) copy-start(f32[64]{0:T(128)} %param.24) | copy-start | bytes 772
  118.6 4.6 %copy-start.12 = (bf16[8,64,256]{2,1,0:T(8,128)(2,1)}, bf16[8,64,256]{2,1,0:T(8,128)(2,1)S(1)}, u32[]{:S(2)}) copy-start(bf16[8,64,256]{2,1,0:T(8,128)(2,1)S(1)} %all-to-all-done.a_ref) | copy-start | bytes 786436
  118.6 37.7 %collective-permute-start.19 = (bf16[4096,128]{1,0:T(8,128)(2,1)}, bf16[4096,128]{1,0:T(8,128)(2,1)}, u32[]{:S(2)}, u32[]{:S(2)}) collective-permute-start(bf16[4096,128]{1,0:T(8,128)(2,1)} %slice.19), channel_id=1, source_target_pairs={{0,2},{2,4},{4,6},{6,8},{8,10},{10,12},{12,14},{14,0},{1,3},{3,5},... | collective-permute-start | bytes 3145736 | tf_op jit(solution)/shard_map/ppermute | solution.py:533
  118.6 37.7 %collective-permute-start.21 = (bf16[4096,128]{1,0:T(8,128)(2,1)}, bf16[4096,128]{1,0:T(8,128)(2,1)S(1)}, u32[]{:S(2)}, u32[]{:S(2)}) collective-permute-start(bf16[4096,128]{1,0:T(8,128)(2,1)} %slice.20), channel_id=1, source_target_pairs={{0,14},{2,0},{4,2},{6,4},{8,6},{10,8},{12,10},{14,12},{1,15},{3,1}... | collective-permute-start | bytes 3145736 | tf_op jit(solution)/shard_map/ppermute | solution.py:533
  121.4 1.8 copy-start.8
  122.3 0.8 copy-start
  129.7 26.6 %all-to-all-start.1 = ((bf16[16,160,128]{2,1,0:T(8,128)(2,1)}), bf16[16,160,128]{2,1,0:T(8,128)(2,1)}, u32[]{:S(2)}, u32[]{:S(2)}) async-start(bf16[16,160,128]{2,1,0:T(8,128)(2,1)} %get-tuple-element.62), calls=%async_computation.1 | async-start | bytes 1310720 | tf_op jit(solution)/shard_map/all_to_all | solution.py:616
  135.1 23.7 %copy-start.1 = (bf16[512,512]{1,0:T(8,128)(2,1)S(1)}, bf16[512,512]{1,0:T(8,128)(2,1)}, u32[]{:S(2)}) copy-start(bf16[512,512]{1,0:T(8,128)(2,1)} %copy-done) | copy-start | bytes 1572868
  136.2 19.3 %collective-permute-start.17 = (bf16[2048,128]{1,0:T(8,128)(2,1)S(1)}, bf16[2048,128]{1,0:T(8,128)(2,1)}, u32[]{:S(2)}, u32[]{:S(2)}) collective-permute-start(bf16[2048,128]{1,0:T(8,128)(2,1)S(1)} %slice.18), channel_id=1, source_target_pairs={{0,2},{2,4},{4,6},{6,8},{8,10},{10,12},{12,14},{14,0},{1,3},{3,5},... | collective-permute-start | bytes 1572872 | tf_op jit(solution)/shard_map/ppermute | solution.py:533
  136.3 19.2 %collective-permute-start.20 = (bf16[2048,128]{1,0:T(8,128)(2,1)S(1)}, bf16[2048,128]{1,0:T(8,128)(2,1)S(1)}, u32[]{:S(2)}, u32[]{:S(2)}) collective-permute-start(bf16[2048,128]{1,0:T(8,128)(2,1)S(1)} %slice.21), channel_id=1, source_target_pairs={{0,14},{2,0},{4,2},{6,4},{8,6},{10,8},{12,10},{14,12},{1,15},{3,1}... | collective-permute-start | bytes 1572872 | tf_op jit(solution)/shard_map/ppermute | solution.py:533
  155.5 0.8 copy-start.6
  156.4 7.7 %copy-start.2 = (bf16[3,2048,128]{2,1,0:T(8,128)(2,1)S(1)}, bf16[3,2048,128]{2,1,0:T(8,128)(2,1)}, u32[]{:S(2)}) copy-start(bf16[3,2048,128]{2,1,0:T(8,128)(2,1)} %bundle.1) | copy-start | bytes 4718596
  156.4 26.4 %collective-permute-start.25 = (bf16[3072,128]{1,0:T(8,128)(2,1)S(1)}, bf16[3072,128]{1,0:T(8,128)(2,1)S(1)}, u32[]{:S(2)}, u32[]{:S(2)}) collective-permute-start(bf16[3072,128]{1,0:T(8,128)(2,1)S(1)} %slice.23), channel_id=1, source_target_pairs={{0,14},{2,0},{4,2},{6,4},{8,6},{10,8},{12,10},{14,12},{1,15},{3,1}... | collective-permute-start | bytes 2359304 | tf_op jit(solution)/shard_map/ppermute | solution.py:533
  160.3 3.8 %collective-permute-start.22 = (bf16[160,2048]{1,0:T(8,128)(2,1)S(1)}, bf16[160,2048]{1,0:T(8,128)(2,1)S(1)}, u32[]{:S(2)}, u32[]{:S(2)}) collective-permute-start(bf16[160,2048]{1,0:T(8,128)(2,1)S(1)} %rows_in.1.own_ref), channel_id=1, source_target_pairs={{0,1},{1,0},{2,3},{3,2},{4,5},{5,4},{6,7},{7,6},{8,9},{9,8},{10,11... | collective-permute-start | bytes 1966088 | tf_op jit(solution)/shard_map/ppermute | solution.py:546
  162.3 20.4 %collective-permute-start.23 = (bf16[2048,128]{1,0:T(8,128)(2,1)}, bf16[2048,128]{1,0:T(8,128)(2,1)S(1)}, u32[]{:S(2)}, u32[]{:S(2)}) collective-permute-start(bf16[2048,128]{1,0:T(8,128)(2,1)} %collective-permute-done.17.refs_5_), channel_id=1, source_target_pairs={{0,2},{2,4},{4,6},{6,8},{8,10},{10,12},{12,14},{14,0},{1,3},{3,5},... | collective-permute-start | bytes 1572872 | tf_op jit(solution)/shard_map/ppermute | solution.py:533
  163.3 19.5 %copy-start.7 = (bf16[2048,128]{1,0:T(8,128)(2,1)S(1)}, bf16[2048,128]{1,0:T(8,128)(2,1)}, u32[]{:S(2)}) copy-start(bf16[2048,128]{1,0:T(8,128)(2,1)} %copy-done.6) | copy-start | bytes 1572868
  163.3 19.4 %collective-permute-start.24 = (bf16[1024,128]{1,0:T(8,128)(2,1)S(1)}, bf16[1024,128]{1,0:T(8,128)(2,1)S(1)}, u32[]{:S(2)}, u32[]{:S(2)}) collective-permute-start(bf16[1024,128]{1,0:T(8,128)(2,1)S(1)} %slice.22), channel_id=1, source_target_pairs={{0,2},{2,4},{4,6},{6,8},{8,10},{10,12},{12,14},{14,0},{1,3},{3,5},... | collective-permute-start | bytes 786440 | tf_op jit(solution)/shard_map/ppermute | solution.py:533
  184.0 2.8 %collective-permute-start.26 = (bf16[160,2048]{1,0:T(8,128)(2,1)S(1)}, bf16[160,2048]{1,0:T(8,128)(2,1)S(1)}, u32[]{:S(2)}, u32[]{:S(2)}) collective-permute-start(bf16[160,2048]{1,0:T(8,128)(2,1)S(1)} %get-tuple-element.69), channel_id=1, source_target_pairs={{0,1},{1,0},{2,3},{3,2},{4,5},{5,4},{6,7},{7,6},{8,9},{9,8},{10,11... | collective-permute-start | bytes 1966088 | tf_op jit(solution)/shard_map/ppermute | solution.py:546
  186.8 17.9 %copy-start.9 = (bf16[64,2048]{1,0:T(8,128)(2,1)S(1)}, bf16[64,2048]{1,0:T(8,128)(2,1)}, u32[]{:S(2)}) copy-start(bf16[64,2048]{1,0:T(8,128)(2,1)} %get-tuple-element.70.upd_ref) | copy-start | bytes 786436
where the time goes:
time: 207 us; the launch traced here: 206 us
  Pallas kernels  64.6 us (31%)
  waiting for transfers between devices  62.6 us (30%)
  starting transfers between devices  50.2 us (24%)
  blocking collectives  17.5 us (8%)
  local copies, waits for them, and re-layouts  9.47 us (5%)
    ppermute x21, waiting for transfers between devices, shift(): lax.ppermute(value, axis, [(i, (i + by) % size) for i in range(size)])  48.6 us
    pallas_call x3, Pallas kernels, attend(): pl.pallas_call(functools.partial(attend_kernel, first, last, count), grid...  36.7 us
    ppermute x21, starting transfers between devices, shift(): lax.ppermute(value, axis, [(i, (i + by) % size) for i in range(size)])  28.7 us
    all_to_all x1, blocking collectives, local(): returned = lax.all_to_all(result, SP, 0, 0, tiled=True)  17.5 us
    all_to_all x1, waiting for transfers between devices, local(): attended = lax.all_to_all(merged, 'z', 0, 0, tiled=True)  8.84 us
    ppermute x4, starting transfers between devices, swap_cores(): return lax.ppermute(value, 'core', ((0, 1), (1, 0)))  7.36 us
    pallas_call x2, Pallas kernels, expert(): pl.pallas_call(functools.partial(expert_kernel, tuple((len(piece) for pie...  7.27 us
    pallas_call x1, Pallas kernels, project(): pl.pallas_call(project_kernel, in_specs=[VMEM, HBM, VMEM, VMEM, VMEM, VME...  6.56 us
  transfers between devices with their start and end apart: 29, of which 13 were waited for; matrix products, arithmetic and copies ran while one was open for 5% of the time, Pallas kernels for 29%

commit v1 on v0

--- a/solution.py
+++ b/solution.py
@@ -119,6 +119,28 @@
         ],
         name="prep",
     )(where, queries, keys, values, query_gain, key_gain, cosine, sine)
+
+
+def stack_kernel(*refs):
+    *parts, out_a, out_b = refs
+    half = len(parts) // 2
+    rows = parts[0].shape[0]
+    for i in range(half):
+        out_a[i * rows : (i + 1) * rows, :] = parts[i][...]
+        out_b[i * rows : (i + 1) * rows, :] = parts[half + i][...]
+
+
+def stack(parts_a, parts_b):
+    rows, width = parts_a[0].shape
+    out = jax.ShapeDtypeStruct((len(parts_a) * rows, width), bf16)
+    return pl.pallas_call(
+        stack_kernel,
+        in_specs=[pl.BlockSpec(memory_space=pltpu.VMEM)] * (2 * len(parts_a)),
+        out_specs=[pl.BlockSpec(memory_space=pltpu.VMEM)] * 2,
+        out_shape=[out, out],
+        compiler_params=room(8),
+        name="stack",
+    )(*parts_a, *parts_b)
 
 
 BQ = 256
@@ -588,8 +610,10 @@
     own, kv_a, kv_b = prep(
         where, queries, keys, values, query_gain[None, :], key_gain[None, :], cosine, sine
     )
-    ax = jnp.concatenate([kv_a] + [shift(kv_a, "x", d) for d in (1, -1, 2)], axis=0)
-    by = jnp.concatenate([kv_b] + [shift(kv_b, "y", d) for d in (1, -1, 2)], axis=0)
+    ax, by = stack(
+        [kv_a] + [shift(kv_a, "x", d) for d in (1, -1, 2)],
+        [kv_b] + [shift(kv_b, "y", d) for d in (1, -1, 2)],
+    )
     sib = swap_cores(own)
     a_next = [shift(ax, "y", 1), shift(ax, "y", -1)]
     b_next = [shift(by, "x", 1), shift(by, "x", -1)]
@@ -610,16 +634,20 @@
     rest_p, rest_m, attended = lax.optimization_barrier((w2p[third:], w2m[third:], attended))
     w3p.append(shift(rest_p, "z", 1))
     w3m.append(shift(rest_m, "z", -1))
+    w4 = [shift(w3p[0][: third // 2], "z", 1), shift(w3m[0][third // 2 :], "z", -1)]
     updated, outgoing = project(
-        attended, out_weight, residual, norm_gain[None, :], route_experts, route_t, swap, peers
+        attended,
+        out_weight,
+        residual,
+        norm_gain[None, :],
+        route_experts,
+        route_t,
+        swap,
+        peers,
     )
     arrived = lax.all_to_all(outgoing, SP, 0, 0, tiled=True)
-    w3p, w3m, arrived = lax.optimization_barrier((w3p, w3m, arrived))
-    w4 = [
-        shift(w3p[0], "z", 1),
-        shift(w3p[1][: third // 2], "z", 1),
-        shift(w3m[1][third // 2 :], "z", -1),
-    ]
+    rest_p, rest_m, arrived = lax.optimization_barrier((w3p[1], w3m[1], arrived))
+    w4 += [shift(rest_p[:third], "z", 1), shift(rest_m[third:], "z", -1)]
     rows = rows_in(arrived, swap)
     sib_rows = swap_cores(rows)
     (acc,) = expert(rows, sib_rows, [[w0], [w1p], [w1m], [w2p], [w2m], w3p], None, False)

time: 207 us -> 192 us (0.928)
  waiting for transfers between devices: 62.6 us -> 31.3 us
  starting transfers between devices: 50.2 us -> 62.8 us
  local copies, waits for them, and re-layouts: 9.47 us -> 13.8 us
    ppermute x21 -> x22, waiting for transfers between devices: 48.6 us -> 14.6 us  [shift(): lax.ppermute(value, axis, [(i, (i + by) % size) for i in range(size)])]
    ppermute x21 -> x22, starting transfers between devices: 28.7 us -> 38.6 us  [shift(): lax.ppermute(value, axis, [(i, (i + by) % size) for i in range(size)])]
    all_to_all x1, waiting for transfers between devices: 0.01 us -> 5.43 us  [local(): arrived = lax.all_to_all(outgoing, SP, 0, 0, tiled=True)]
    ppermute x4, starting transfers between devices: 7.36 us -> 10.5 us  [swap_cores(): return lax.ppermute(value, 'core', ((0, 1), (1, 0)))]
    slice x2 -> x4, local copies, waits for them, and re-layouts: 1.02 us -> 3.14 us  [the longest x2 2.15 us: local(): w4 += [shift(rest_p[:third], 'z', 1), shift(rest_m[third:], 'z', -1)]]
    unnamed x38 -> x32, local copies, waits for them, and re-layouts: 3.76 us -> 4.49 us
  transfers between devices with their start and end apart: 29 -> 30, of which waited for: 13 -> 10; matrix products, arithmetic and copies ran while one was open for 5% -> 6% of each run, Pallas kernels for 29% -> 30%
where the time goes in v1:
time: 192 us
  Pallas kernels  63.8 us (33%)
  starting transfers between devices  62.8 us (33%)
  waiting for transfers between devices  31.3 us (16%)
  blocking collectives  18.2 us (9%)
  local copies, waits for them, and re-layouts  13.8 us (7%)
    ppermute x22, starting transfers between devices, shift(): lax.ppermute(value, axis, [(i, (i + by) % size) for i in range(size)])  38.6 us
    pallas_call x3, Pallas kernels, attend(): pl.pallas_call(functools.partial(attend_kernel, first, last, count), grid...  35.6 us
    all_to_all x1, blocking collectives, local(): returned = lax.all_to_all(result, SP, 0, 0, tiled=True)  18.2 us
    ppermute x22, waiting for transfers between devices, shift(): lax.ppermute(value, axis, [(i, (i + by) % size) for i in range(size)])  14.6 us
    ppermute x4, starting transfers between devices, swap_cores(): return lax.ppermute(value, 'core', ((0, 1), (1, 0)))  10.5 us
    pallas_call x2, Pallas kernels, expert(): pl.pallas_call(functools.partial(expert_kernel, tuple((len(piece) for pie...  8.5 us
    all_to_all x1, waiting for transfers between devices, local(): attended = lax.all_to_all(merged, 'z', 0, 0, tiled=True)  7.76 us
    pallas_call x1, Pallas kernels, project(): pl.pallas_call(project_kernel, in_specs=[VMEM, HBM, VMEM, VMEM, VMEM, VME...  6.53 us
  transfers between devices with their start and end apart: 30, of which 10 were waited for; matrix products, arithmetic and copies ran while one was open for 6% of the time, Pallas kernels for 30%

profile of v1, /device:TPU:1, one launch (start us, length us, event | category | flops | bytes accessed | tf_op | source)
XLA Modules:
  0.0 191.8 jit_solution(16953569575159242710)
XLA Ops:
  0.0 2.4 %bundle.1 = bf16[3,2048,128]{2,1,0:T(8,128)(2,1)} custom-call(bf16[2048,128]{1,0:T(8,128)(2,1)} %bitcast.16, bf16[2048,128]{1,0:T(8,128)(2,1)} %bitcast.17, bf16[128,2048]{1,0:T(8,128)(2,1)} %bitcast.18), custom_call_target="tpu_custom_call" | custom-call | tf_op jit(solution)/shard_map/bundle/pallas_call | solution.py:43
  2.4 2.5 %collective-permute-start = (bf16[6144,128]{1,0:T(8,128)(2,1)}, bf16[6144,128]{1,0:T(8,128)(2,1)}, u32[]{:S(2)}, u32[]{:S(2)}) collective-permute-start(bf16[6144,128]{1,0:T(8,128)(2,1)} %bitcast.11), channel_id=1, source_target_pairs={{0,2},{2,4},{4,6},{6,8},{8,10},{10,12},{12,14},{14,0},{1,3},{3,5},... | collective-permute-start | bytes 4718600 | tf_op jit(solution)/shard_map/ppermute | solution.py:555
  4.8 3.9 %collective-permute-start.1 = (bf16[6144,128]{1,0:T(8,128)(2,1)}, bf16[6144,128]{1,0:T(8,128)(2,1)}, u32[]{:S(2)}, u32[]{:S(2)}) collective-permute-start(bf16[6144,128]{1,0:T(8,128)(2,1)} %bitcast.12), channel_id=1, source_target_pairs={{0,14},{2,0},{4,2},{6,4},{8,6},{10,8},{12,10},{14,12},{1,15},{3,1}... | collective-permute-start | bytes 4718600 | tf_op jit(solution)/shard_map/ppermute | solution.py:555
  8.8 0.6 pad_add_fusion.where_ref
  9.4 0.9 fusion
  10.3 5.3 %prep.1 = (bf16[1024,128]{1,0:T(8,128)(2,1)}, bf16[256,256]{1,0:T(8,128)(2,1)}, bf16[256,256]{1,0:T(8,128)(2,1)}) custom-call(s32[2]{0:T(128)} %pad_add_fusion.where_ref, bf16[1024,128]{1,0:T(8,128)(2,1)} %q_ref.1, bf16[1024,512]{1,0:T(8,128)(2,1)} %k_ref.1, bf16[1024,512]{1,0:T(8,128)(2,1)} %v_ref.1, f32[1,128]{1,0:T(1,128)} %bitcast.20, ...), custom_call_target="tpu_custom_call" | custom-call | tf_op jit(solution)/shard_map/prep/pallas_call | solution.py:95
  15.6 1.2 collective-permute-start.3
  16.8 1.5 collective-permute-start.4
  18.2 1.5 collective-permute-start.5
  19.8 1.4 collective-permute-done.3.refs_1_
  21.2 1.3 collective-permute-start.6
  22.5 1.4 collective-permute-start.7
  23.9 1.2 collective-permute-done.5.refs_3_
  25.2 2.9 %collective-permute-start.8 = (bf16[256,256]{1,0:T(8,128)(2,1)}, bf16[256,256]{1,0:T(8,128)(2,1)S(1)}, u32[]{:S(2)}, u32[]{:S(2)}) collective-permute-start(bf16[256,256]{1,0:T(8,128)(2,1)} %get-tuple-element.41.refs_4_), channel_id=1, source_target_pairs={{0,128},{64,192},{128,0},{192,64},{1,129},{65,193},{129,1},{193,65... | collective-permute-start | bytes 393224 | tf_op jit(solution)/shard_map/ppermute | solution.py:555
  28.1 3.2 %collective-permute-done.8.refs_7_ = bf16[256,256]{1,0:T(8,128)(2,1)S(1)} collective-permute-done((bf16[256,256]{1,0:T(8,128)(2,1)}, bf16[256,256]{1,0:T(8,128)(2,1)S(1)}, u32[]{:S(2)}, u32[]{:S(2)}) %collective-permute-start.8) | collective-permute-done | bytes 131104 | tf_op jit(solution)/shard_map/ppermute | solution.py:555
  31.2 0.9 copy-done.8
  32.2 0.9 copy-done.9
  33.1 2.4 %collective-permute-start.10 = (bf16[1024,256]{1,0:T(8,128)(2,1)S(1)}, bf16[1024,256]{1,0:T(8,128)(2,1)S(1)}, u32[]{:S(2)}, u32[]{:S(2)}) collective-permute-start(bf16[1024,256]{1,0:T(8,128)(2,1)S(1)} %get-tuple-element.42.refs_0_), channel_id=1, source_target_pairs={{0,192},{64,0},{128,64},{192,128},{1,193},{65,1},{129,65},{193,129... | collective-permute-start | bytes 1572872 | tf_op jit(solution)/shard_map/ppermute | solution.py:555
  35.5 3.1 %collective-permute-start.2 = (bf16[1024,128]{1,0:T(8,128)(2,1)}, bf16[1024,128]{1,0:T(8,128)(2,1)S(1)}, u32[]{:S(2)}, u32[]{:S(2)}) collective-permute-start(bf16[1024,128]{1,0:T(8,128)(2,1)} %get-tuple-element.39.own_ref), channel_id=1, source_target_pairs={{0,1},{1,0},{2,3},{3,2},{4,5},{5,4},{6,7},{7,6},{8,9},{9,8},{10,11... | collective-permute-start | bytes 786440 | tf_op jit(solution)/shard_map/ppermute | solution.py:568
  38.6 1.1 collective-permute-start.11
  39.7 0.2 collective-permute-done.2.sib_ref
  40.0 2.9 %collective-permute-start.12 = (bf16[1024,256]{1,0:T(8,128)(2,1)S(1)}, bf16[1024,256]{1,0:T(8,128)(2,1)S(1)}, u32[]{:S(2)}, u32[]{:S(2)}) collective-permute-start(bf16[1024,256]{1,0:T(8,128)(2,1)S(1)} %get-tuple-element.43.refs_1_), channel_id=1, source_target_pairs={{0,48},{16,0},{32,16},{48,32},{1,49},{17,1},{33,17},{49,33},{2,50}... | collective-permute-start | bytes 1572872 | tf_op jit(solution)/shard_map/ppermute | solution.py:555
  42.9 1.7 collective-permute-done.10.refs_1_
  44.6 2.3 %collective-permute-start.9 = (bf16[1024,256]{1,0:T(8,128)(2,1)S(1)}, bf16[1024,256]{1,0:T(8,128)(2,1)S(1)}, u32[]{:S(2)}, u32[]{:S(2)}) collective-permute-start(bf16[1024,256]{1,0:T(8,128)(2,1)S(1)} %get-tuple-element.42.refs_0_), channel_id=1, source_target_pairs={{0,64},{64,128},{128,192},{192,0},{1,65},{65,129},{129,193},{193,1... | collective-permute-start | bytes 1572872 | tf_op jit(solution)/shard_map/ppermute | solution.py:555
  46.9 0.9 copy-done.3
  47.8 10.1 %attend.3 = (f32[2,1024,256]{2,1,0:T(8,128)S(1)}, f32[2,1024,128]{2,1,0:T(8,128)S(1)}) custom-call(s32[2]{0:T(128)S(1)} %copy-done.10, bf16[1024,128]{1,0:T(8,128)(2,1)S(1)} %copy-done.3, bf16[1024,128]{1,0:T(8,128)(2,1)S(1)} %collective-permute-done.2.sib_ref, bf16[1024,256]{1,0:T(8,128)(2,1)S(1)} %get-tuple-element.42.refs_0_, ...), custom_call_target="tpu_custom_call" | custom-call | tf_op jit(solution)/shard_map/attend/pallas_call | solution.py:228
  58.1 0.7 copy-done.4
  58.8 2.7 %collective-permute-start.14 = (bf16[6144,128]{1,0:T(8,128)(2,1)}, bf16[6144,128]{1,0:T(8,128)(2,1)}, u32[]{:S(2)}, u32[]{:S(2)}) collective-permute-start(bf16[6144,128]{1,0:T(8,128)(2,1)} %collective-permute-done.1.refs_2_), channel_id=1, source_target_pairs={{0,14},{2,0},{4,2},{6,4},{8,6},{10,8},{12,10},{14,12},{1,15},{3,1}... | collective-permute-start | bytes 4718600 | tf_op jit(solution)/shard_map/ppermute | solution.py:555
  61.5 2.4 %collective-permute-start.15 = (bf16[1024,256]{1,0:T(8,128)(2,1)S(1)}, bf16[1024,256]{1,0:T(8,128)(2,1)S(1)}, u32[]{:S(2)}, u32[]{:S(2)}) collective-permute-start(bf16[1024,256]{1,0:T(8,128)(2,1)S(1)} %broadcast_select_fusion.1), channel_id=1, source_target_pairs={{0,64},{1,193},{64,128},{65,1},{128,192},{129,65},{192,0},{193,129... | collective-permute-start | bytes 1572872 | tf_op jit(solution)/shard_map/ppermute | solution.py:564
  64.0 15.1 %attend.4 = (f32[2,1024,256]{2,1,0:T(8,128)S(1)}, f32[2,1024,128]{2,1,0:T(8,128)S(1)}) custom-call(s32[2]{0:T(128)S(1)} %copy-done.10, bf16[1024,128]{1,0:T(8,128)(2,1)S(1)} %copy-done.3, bf16[1024,128]{1,0:T(8,128)(2,1)S(1)} %collective-permute-done.2.sib_ref, bf16[1024,256]{1,0:T(8,128)(2,1)S(1)} %collective-permute-done.9.refs_0_, ...), custom_call_target="tpu_custom_call" | custom-call | tf_op jit(solution)/shard_map/attend/pallas_call | solution.py:228
  79.1 10.3 %attend.5 = (f32[2,8,64,256]{3,2,1,0:T(8,128)S(1)}, bf16[2,8,64,256]{3,2,1,0:T(8,128)(2,1)S(1)}) custom-call(s32[2]{0:T(128)S(1)} %copy-done.10, bf16[1024,128]{1,0:T(8,128)(2,1)S(1)} %copy-done.3, bf16[1024,128]{1,0:T(8,128)(2,1)S(1)} %collective-permute-done.2.sib_ref, bf16[1024,256]{1,0:T(8,128)(2,1)S(1)} %collective-permute-done.15.refs_0_, ...), custom_call_target="tpu_custom_call" | custom-call | tf_op jit(solution)/shard_map/attend/pallas_call | solution.py:228
  89.5 2.6 %collective-permute-start.17 = (bf16[2,8,64,256]{3,2,1,0:T(8,128)(2,1)S(1)}, bf16[2,8,64,256]{3,2,1,0:T(8,128)(2,1)S(1)}, u32[]{:S(2)}, u32[]{:S(2)}) collective-permute-start(bf16[2,8,64,256]{3,2,1,0:T(8,128)(2,1)S(1)} %get-tuple-element.59), channel_id=1, source_target_pairs={{0,1},{1,0},{2,3},{3,2},{4,5},{5,4},{6,7},{7,6},{8,9},{9,8},{10,11... | collective-permute-start | bytes 1572872 | tf_op jit(solution)/shard_map/ppermute | solution.py:568
  92.1 1.5 collective-permute-done.17.got_ref
  93.6 2.3 %merge.1 = bf16[8,64,256]{2,1,0:T(8,128)(2,1)} custom-call(s32[2]{0:T(128)S(1)} %copy-done.10, f32[2,8,64,256]{3,2,1,0:T(8,128)S(1)} %get-tuple-element.56.keep_ref, bf16[2,8,64,256]{3,2,1,0:T(8,128)(2,1)S(1)} %collective-permute-done.17.got_ref), custom_call_target="tpu_custom_call" | custom-call | tf_op jit(solution)/shard_map/merge/pallas_call | solution.py:268
  95.9 5.1 %all-to-all-start = ((bf16[8,64,256]{2,1,0:T(8,128)(2,1)}), bf16[8,64,256]{2,1,0:T(8,128)(2,1)S(1)}, u32[]{:S(2)}, u32[]{:S(2)}) async-start(bf16[8,64,256]{2,1,0:T(8,128)(2,1)} %merge.1), calls=%async_computation | async-start | bytes 524288 | tf_op jit(solution)/shard_map/all_to_all | solution.py:633
  101.0 1.0 slice.24
  102.1 2.3 %slice.25 = bf16[4096,128]{1,0:T(8,128)(2,1)} slice(bf16[6144,128]{1,0:T(8,128)(2,1)} %collective-permute-done.14.refs_4_), slice={[2048:6144], [0:128]} | slice | bytes 2097152 | tf_op jit(solution)/shard_map/slice | solution.py:634
  104.4 7.8 %all-to-all-done.a_ref = bf16[8,64,256]{2,1,0:T(8,128)(2,1)S(1)} async-done(((bf16[8,64,256]{2,1,0:T(8,128)(2,1)}), bf16[8,64,256]{2,1,0:T(8,128)(2,1)S(1)}, u32[]{:S(2)}, u32[]{:S(2)}) %all-to-all-start) | async-done | bytes 262176 | tf_op jit(solution)/shard_map/all_to_all | solution.py:633
  112.1 2.7 %collective-permute-start.19 = (bf16[4096,128]{1,0:T(8,128)(2,1)}, bf16[4096,128]{1,0:T(8,128)(2,1)}, u32[]{:S(2)}, u32[]{:S(2)}) collective-permute-start(bf16[4096,128]{1,0:T(8,128)(2,1)} %slice.25), channel_id=1, source_target_pairs={{0,14},{2,0},{4,2},{6,4},{8,6},{10,8},{12,10},{14,12},{1,15},{3,1}... | collective-permute-start | bytes 3145736 | tf_op jit(solution)/shard_map/ppermute | solution.py:555
  114.8 0.1 copy.18.route_ref
  114.9 0.1 copy.16.score_ref
  115.1 0.7 plan.1
  115.9 0.8 copy-done
  116.7 6.5 %project.1 = (bf16[64,2048]{1,0:T(8,128)(2,1)}, bf16[16,160,128]{2,1,0:T(8,128)(2,1)}) custom-call(bf16[8,64,256]{2,1,0:T(8,128)(2,1)} %copy-done.12, bf16[2048,2048]{1,0:T(8,128)(2,1)} %w_ref.1, bf16[64,2048]{1,0:T(8,128)(2,1)} %res_ref.1, f32[1,2048]{1,0:T(1,128)} %bitcast.19, s32[64,2]{1,0:T(8,128)} %copy-done.6, s32[2,64]{1,0:T(2,128)} %bitcast.14, ...), custom_call_target="tpu_custom_call" | custom-call | tf_op jit(solution)/shard_map/project/pallas_call | solution.py:363
  123.2 6.1 %all-to-all-start.1 = ((bf16[16,160,128]{2,1,0:T(8,128)(2,1)}), bf16[16,160,128]{2,1,0:T(8,128)(2,1)S(1)}, u32[]{:S(2)}, u32[]{:S(2)}) async-start(bf16[16,160,128]{2,1,0:T(8,128)(2,1)} %get-tuple-element.64), calls=%async_computation.1 | async-start | bytes 1310720 | tf_op jit(solution)/shard_map/all_to_all | solution.py:648
  129.4 0.9 slice.27
  130.3 1.9 slice.26
  132.1 2.7 %collective-permute-start.21 = (bf16[2048,128]{1,0:T(8,128)(2,1)}, bf16[2048,128]{1,0:T(8,128)(2,1)S(1)}, u32[]{:S(2)}, u32[]{:S(2)}) collective-permute-start(bf16[2048,128]{1,0:T(8,128)(2,1)} %slice.26), channel_id=1, source_target_pairs={{0,14},{2,0},{4,2},{6,4},{8,6},{10,8},{12,10},{14,12},{1,15},{3,1}... | collective-permute-start | bytes 1572872 | tf_op jit(solution)/shard_map/ppermute | solution.py:555
  134.8 5.4 %all-to-all-done.1.in_ref = bf16[16,160,128]{2,1,0:T(8,128)(2,1)S(1)} async-done(((bf16[16,160,128]{2,1,0:T(8,128)(2,1)}), bf16[16,160,128]{2,1,0:T(8,128)(2,1)S(1)}, u32[]{:S(2)}, u32[]{:S(2)}) %all-to-all-start.1) | async-done | bytes 655392 | tf_op jit(solution)/shard_map/all_to_all | solution.py:648
  140.2 0.3 rows_in.1.own_ref
  140.6 3.2 %collective-permute-start.20 = (bf16[160,2048]{1,0:T(8,128)(2,1)S(1)}, bf16[160,2048]{1,0:T(8,128)(2,1)S(1)}, u32[]{:S(2)}, u32[]{:S(2)}) collective-permute-start(bf16[160,2048]{1,0:T(8,128)(2,1)S(1)} %rows_in.1.own_ref), channel_id=1, source_target_pairs={{0,1},{1,0},{2,3},{3,2},{4,5},{5,4},{6,7},{7,6},{8,9},{9,8},{10,11... | collective-permute-start | bytes 1966088 | tf_op jit(solution)/shard_map/ppermute | solution.py:568
  143.8 1.1 slice.30
  145.0 1.1 slice.31
  146.0 2.7 %collective-permute-start.26 = (bf16[2048,128]{1,0:T(8,128)(2,1)S(1)}, bf16[2048,128]{1,0:T(8,128)(2,1)S(1)}, u32[]{:S(2)}, u32[]{:S(2)}) collective-permute-start(bf16[2048,128]{1,0:T(8,128)(2,1)S(1)} %slice.31), channel_id=1, source_target_pairs={{0,14},{2,0},{4,2},{6,4},{8,6},{10,8},{12,10},{14,12},{1,15},{3,1}... | collective-permute-start | bytes 1572872 | tf_op jit(solution)/shard_map/ppermute | solution.py:555
  148.8 1.0 slice.32
  149.9 2.7 %collective-permute-start.24 = (bf16[1024,128]{1,0:T(8,128)(2,1)S(1)}, bf16[1024,128]{1,0:T(8,128)(2,1)S(1)}, u32[]{:S(2)}, u32[]{:S(2)}) collective-permute-start(bf16[1024,128]{1,0:T(8,128)(2,1)S(1)} %slice.33), channel_id=1, source_target_pairs={{0,14},{2,0},{4,2},{6,4},{8,6},{10,8},{12,10},{14,12},{1,15},{3,1}... | collective-permute-start | bytes 786440 | tf_op jit(solution)/shard_map/ppermute | solution.py:555
  152.6 6.0 %expert.2.refs_6_ = f32[320,2048]{1,0:T(8,128)S(1)} custom-call(bf16[160,2048]{1,0:T(8,128)(2,1)S(1)} %rows_in.1.own_ref, bf16[160,2048]{1,0:T(8,128)(2,1)S(1)} %collective-permute-done.20.sib_ref, bf16[6144,128]{1,0:T(8,128)(2,1)S(1)} %bitcast.13, bf16[6144,128]{1,0:T(8,128)(2,1)} %collective-permute-done.refs_1_, ...), custom_call_target="tpu_custom_call" | custom-call | tf_op jit(solution)/shard_map/expert/pallas_call | solution.py:459
  158.6 7.1 %collective-permute-done.23.refs_2_ = bf16[1024,128]{1,0:T(8,128)(2,1)S(1)} collective-permute-done((bf16[1024,128]{1,0:T(8,128)(2,1)S(1)}, bf16[1024,128]{1,0:T(8,128)(2,1)S(1)}, u32[]{:S(2)}, u32[]{:S(2)}) %collective-permute-start.23) | collective-permute-done | bytes 262176 | tf_op jit(solution)/shard_map/ppermute | solution.py:555
  165.7 2.5 %expert.3 = (f32[160,2048]{1,0:T(8,128)S(1)}, bf16[160,2048]{1,0:T(8,128)(2,1)S(1)}) custom-call(bf16[160,2048]{1,0:T(8,128)(2,1)S(1)} %rows_in.1.own_ref, bf16[160,2048]{1,0:T(8,128)(2,1)S(1)} %collective-permute-done.20.sib_ref, bf16[2048,128]{1,0:T(8,128)(2,1)S(1)} %collective-permute-done.21.refs_0_, bf16[4096,128]{1,0:T(8,128)(2,1)} %collective-permute-done.19.refs_1_, ...), custom_call_target="tpu_custom_call" | custom-call | tf_op jit(solution)/shard_map/expert/pallas_call | solution.py:459
  168.2 1.6 collective-permute-start.27
  169.8 1.7 collective-permute-done.27.got_ref
  171.5 0.4 finish.1
  172.0 18.2 %all_to_all.15.in_ref = bf16[16,160,128]{2,1,0:T(8,128)(2,1)S(1)} all-to-all(bf16[16,160,128]{2,1,0:T(8,128)(2,1)S(1)} %finish.1), channel_id=1, replica_groups=mesh['y'=4,'x'=4,'z'=8,'core'=2] {'y','x'}, dimensions={0} | all-to-all | bytes 1310720 | tf_op jit(solution)/shard_map/all_to_all | solution.py:656
  190.2 1.6 mix.1
  (58 shorter events, 0.6 us)
Async XLA Ops:
  2.4 55.6 %collective-permute-start = (bf16[6144,128]{1,0:T(8,128)(2,1)}, bf16[6144,128]{1,0:T(8,128)(2,1)}, u32[]{:S(2)}, u32[]{:S(2)}) collective-permute-start(bf16[6144,128]{1,0:T(8,128)(2,1)} %bitcast.11), channel_id=1, source_target_pairs={{0,2},{2,4},{4,6},{6,8},{8,10},{10,12},{12,14},{14,0},{1,3},{3,5},... | collective-permute-start | bytes 4718600 | tf_op jit(solution)/shard_map/ppermute | solution.py:555
  4.8 53.2 %collective-permute-start.1 = (bf16[6144,128]{1,0:T(8,128)(2,1)}, bf16[6144,128]{1,0:T(8,128)(2,1)}, u32[]{:S(2)}, u32[]{:S(2)}) collective-permute-start(bf16[6144,128]{1,0:T(8,128)(2,1)} %bitcast.12), channel_id=1, source_target_pairs={{0,14},{2,0},{4,2},{6,4},{8,6},{10,8},{12,10},{14,12},{1,15},{3,1}... | collective-permute-start | bytes 4718600 | tf_op jit(solution)/shard_map/ppermute | solution.py:555
  10.3 36.6 %copy-start.10 = (s32[2]{0:T(128)S(1)}, s32[2]{0:T(128)}, u32[]{:S(2)}) copy-start(s32[2]{0:T(128)} %pad_add_fusion.where_ref) | copy-start | bytes 28
  15.6 5.6 %collective-permute-start.3 = (bf16[256,256]{1,0:T(8,128)(2,1)}, bf16[256,256]{1,0:T(8,128)(2,1)S(1)}, u32[]{:S(2)}, u32[]{:S(2)}) collective-permute-start(bf16[256,256]{1,0:T(8,128)(2,1)} %get-tuple-element.40.refs_0_), channel_id=1, source_target_pairs={{0,16},{16,32},{32,48},{48,0},{1,17},{17,33},{33,49},{49,1},{2,18}... | collective-permute-start | bytes 393224 | tf_op jit(solution)/shard_map/ppermute | solution.py:555
  16.8 5.7 %collective-permute-start.4 = (bf16[256,256]{1,0:T(8,128)(2,1)}, bf16[256,256]{1,0:T(8,128)(2,1)S(1)}, u32[]{:S(2)}, u32[]{:S(2)}) collective-permute-start(bf16[256,256]{1,0:T(8,128)(2,1)} %get-tuple-element.40.refs_0_), channel_id=1, source_target_pairs={{0,48},{16,0},{32,16},{48,32},{1,49},{17,1},{33,17},{49,33},{2,50}... | collective-permute-start | bytes 393224 | tf_op jit(solution)/shard_map/ppermute | solution.py:555
  18.2 6.9 %collective-permute-start.5 = (bf16[256,256]{1,0:T(8,128)(2,1)}, bf16[256,256]{1,0:T(8,128)(2,1)S(1)}, u32[]{:S(2)}, u32[]{:S(2)}) collective-permute-start(bf16[256,256]{1,0:T(8,128)(2,1)} %get-tuple-element.40.refs_0_), channel_id=1, source_target_pairs={{0,32},{16,48},{32,0},{48,16},{1,33},{17,49},{33,1},{49,17},{2,34}... | collective-permute-start | bytes 393224 | tf_op jit(solution)/shard_map/ppermute | solution.py:555
  21.2 6.9 %collective-permute-start.6 = (bf16[256,256]{1,0:T(8,128)(2,1)}, bf16[256,256]{1,0:T(8,128)(2,1)S(1)}, u32[]{:S(2)}, u32[]{:S(2)}) collective-permute-start(bf16[256,256]{1,0:T(8,128)(2,1)} %get-tuple-element.41.refs_4_), channel_id=1, source_target_pairs={{0,64},{64,128},{128,192},{192,0},{1,65},{65,129},{129,193},{193,1... | collective-permute-start | bytes 393224 | tf_op jit(solution)/shard_map/ppermute | solution.py:555
  22.5 5.6 %collective-permute-start.7 = (bf16[256,256]{1,0:T(8,128)(2,1)}, bf16[256,256]{1,0:T(8,128)(2,1)S(1)}, u32[]{:S(2)}, u32[]{:S(2)}) collective-permute-start(bf16[256,256]{1,0:T(8,128)(2,1)} %get-tuple-element.41.refs_4_), channel_id=1, source_target_pairs={{0,192},{64,0},{128,64},{192,128},{1,193},{65,1},{129,65},{193,129... | collective-permute-start | bytes 393224 | tf_op jit(solution)/shard_map/ppermute | solution.py:555
  25.2 6.1 %collective-permute-start.8 = (bf16[256,256]{1,0:T(8,128)(2,1)}, bf16[256,256]{1,0:T(8,128)(2,1)S(1)}, u32[]{:S(2)}, u32[]{:S(2)}) collective-permute-start(bf16[256,256]{1,0:T(8,128)(2,1)} %get-tuple-element.41.refs_4_), channel_id=1, source_target_pairs={{0,128},{64,192},{128,0},{192,64},{1,129},{65,193},{129,1},{193,65... | collective-permute-start | bytes 393224 | tf_op jit(solution)/shard_map/ppermute | solution.py:555
  31.2 0.9 copy-start.8
  32.2 0.9 copy-start.9
  33.1 11.4 %collective-permute-start.10 = (bf16[1024,256]{1,0:T(8,128)(2,1)S(1)}, bf16[1024,256]{1,0:T(8,128)(2,1)S(1)}, u32[]{:S(2)}, u32[]{:S(2)}) collective-permute-start(bf16[1024,256]{1,0:T(8,128)(2,1)S(1)} %get-tuple-element.42.refs_0_), channel_id=1, source_target_pairs={{0,192},{64,0},{128,64},{192,128},{1,193},{65,1},{129,65},{193,129... | collective-permute-start | bytes 1572872 | tf_op jit(solution)/shard_map/ppermute | solution.py:555
  35.5 4.5 %collective-permute-start.2 = (bf16[1024,128]{1,0:T(8,128)(2,1)}, bf16[1024,128]{1,0:T(8,128)(2,1)S(1)}, u32[]{:S(2)}, u32[]{:S(2)}) collective-permute-start(bf16[1024,128]{1,0:T(8,128)(2,1)} %get-tuple-element.39.own_ref), channel_id=1, source_target_pairs={{0,1},{1,0},{2,3},{3,2},{4,5},{5,4},{6,7},{7,6},{8,9},{9,8},{10,11... | collective-permute-start | bytes 786440 | tf_op jit(solution)/shard_map/ppermute | solution.py:568
  38.6 19.4 %collective-permute-start.11 = (bf16[1024,256]{1,0:T(8,128)(2,1)S(1)}, bf16[1024,256]{1,0:T(8,128)(2,1)S(1)}, u32[]{:S(2)}, u32[]{:S(2)}) collective-permute-start(bf16[1024,256]{1,0:T(8,128)(2,1)S(1)} %get-tuple-element.43.refs_1_), channel_id=1, source_target_pairs={{0,16},{16,32},{32,48},{48,0},{1,17},{17,33},{33,49},{49,1},{2,18}... | collective-permute-start | bytes 1572872 | tf_op jit(solution)/shard_map/ppermute | solution.py:555
  40.0 18.0 %collective-permute-start.12 = (bf16[1024,256]{1,0:T(8,128)(2,1)S(1)}, bf16[1024,256]{1,0:T(8,128)(2,1)S(1)}, u32[]{:S(2)}, u32[]{:S(2)}) collective-permute-start(bf16[1024,256]{1,0:T(8,128)(2,1)S(1)} %get-tuple-element.43.refs_1_), channel_id=1, source_target_pairs={{0,48},{16,0},{32,16},{48,32},{1,49},{17,1},{33,17},{49,33},{2,50}... | collective-permute-start | bytes 1572872 | tf_op jit(solution)/shard_map/ppermute | solution.py:555
  44.6 13.4 %collective-permute-start.9 = (bf16[1024,256]{1,0:T(8,128)(2,1)S(1)}, bf16[1024,256]{1,0:T(8,128)(2,1)S(1)}, u32[]{:S(2)}, u32[]{:S(2)}) collective-permute-start(bf16[1024,256]{1,0:T(8,128)(2,1)S(1)} %get-tuple-element.42.refs_0_), channel_id=1, source_target_pairs={{0,64},{64,128},{128,192},{192,0},{1,65},{65,129},{129,193},{193,1... | collective-permute-start | bytes 1572872 | tf_op jit(solution)/shard_map/ppermute | solution.py:555
  46.9 1.0 copy-start.3
  58.0 0.8 copy-start.4
  58.8 20.3 %collective-permute-start.16 = (bf16[1024,256]{1,0:T(8,128)(2,1)S(1)}, bf16[1024,256]{1,0:T(8,128)(2,1)S(1)}, u32[]{:S(2)}, u32[]{:S(2)}) collective-permute-start(bf16[1024,256]{1,0:T(8,128)(2,1)S(1)} %broadcast_select_fusion), channel_id=1, source_target_pairs={{0,16},{1,49},{16,32},{17,1},{32,48},{33,17},{48,0},{49,33},{2,18}... | collective-permute-start | bytes 1572872 | tf_op jit(solution)/shard_map/ppermute | solution.py:564
  58.8 5.2 %copy-start.5 = (bf16[1024,256]{1,0:T(8,128)(2,1)S(1)}, bf16[1024,256]{1,0:T(8,128)(2,1)}, u32[]{:S(2)}) copy-start(bf16[1024,256]{1,0:T(8,128)(2,1)} %copy-done.4) | copy-start | bytes 1572868
  58.8 42.2 %collective-permute-start.13 = (bf16[6144,128]{1,0:T(8,128)(2,1)}, bf16[6144,128]{1,0:T(8,128)(2,1)S(1)}, u32[]{:S(2)}, u32[]{:S(2)}) collective-permute-start(bf16[6144,128]{1,0:T(8,128)(2,1)} %collective-permute-done.refs_1_), channel_id=1, source_target_pairs={{0,2},{2,4},{4,6},{6,8},{8,10},{10,12},{12,14},{14,0},{1,3},{3,5},... | collective-permute-start | bytes 4718600 | tf_op jit(solution)/shard_map/ppermute | solution.py:555
  58.8 42.2 %collective-permute-start.14 = (bf16[6144,128]{1,0:T(8,128)(2,1)}, bf16[6144,128]{1,0:T(8,128)(2,1)}, u32[]{:S(2)}, u32[]{:S(2)}) collective-permute-start(bf16[6144,128]{1,0:T(8,128)(2,1)} %collective-permute-done.1.refs_2_), channel_id=1, source_target_pairs={{0,14},{2,0},{4,2},{6,4},{8,6},{10,8},{12,10},{14,12},{1,15},{3,1}... | collective-permute-start | bytes 4718600 | tf_op jit(solution)/shard_map/ppermute | solution.py:555
  61.5 17.6 %collective-permute-start.15 = (bf16[1024,256]{1,0:T(8,128)(2,1)S(1)}, bf16[1024,256]{1,0:T(8,128)(2,1)S(1)}, u32[]{:S(2)}, u32[]{:S(2)}) collective-permute-start(bf16[1024,256]{1,0:T(8,128)(2,1)S(1)} %broadcast_select_fusion.1), channel_id=1, source_target_pairs={{0,64},{1,193},{64,128},{65,1},{128,192},{129,65},{192,0},{193,129... | collective-permute-start | bytes 1572872 | tf_op jit(solution)/shard_map/ppermute | solution.py:564
  89.5 4.1 %collective-permute-start.17 = (bf16[2,8,64,256]{3,2,1,0:T(8,128)(2,1)S(1)}, bf16[2,8,64,256]{3,2,1,0:T(8,128)(2,1)S(1)}, u32[]{:S(2)}, u32[]{:S(2)}) collective-permute-start(bf16[2,8,64,256]{3,2,1,0:T(8,128)(2,1)S(1)} %get-tuple-element.59), channel_id=1, source_target_pairs={{0,1},{1,0},{2,3},{3,2},{4,5},{5,4},{6,7},{7,6},{8,9},{9,8},{10,11... | collective-permute-start | bytes 1572872 | tf_op jit(solution)/shard_map/ppermute | solution.py:568
  95.9 16.2 %all-to-all-start = ((bf16[8,64,256]{2,1,0:T(8,128)(2,1)}), bf16[8,64,256]{2,1,0:T(8,128)(2,1)S(1)}, u32[]{:S(2)}, u32[]{:S(2)}) async-start(bf16[8,64,256]{2,1,0:T(8,128)(2,1)} %merge.1), calls=%async_computation | async-start | bytes 524288 | tf_op jit(solution)/shard_map/all_to_all | solution.py:633
  102.1 12.7 %copy-start.11 = (s32[64,2]{0,1:T(2,128)S(1)}, s32[64,2]{0,1:T(2,128)}, u32[]{:S(2)}) copy-start(s32[64,2]{0,1:T(2,128)} %param.22) | copy-start | bytes 1540
  102.1 12.8 %copy-start.13 = (f32[64,2]{0,1:T(2,128)S(1)}, f32[64,2]{0,1:T(2,128)}, u32[]{:S(2)}) copy-start(f32[64,2]{0,1:T(2,128)} %param.23) | copy-start | bytes 1540
  102.1 12.9 %copy-start.14 = (f32[64]{0:T(128)S(1)}, f32[64]{0:T(128)}, u32[]{:S(2)}) copy-start(f32[64]{0:T(128)} %param.24) | copy-start | bytes 772
  112.1 4.6 %copy-start.12 = (bf16[8,64,256]{2,1,0:T(8,128)(2,1)}, bf16[8,64,256]{2,1,0:T(8,128)(2,1)S(1)}, u32[]{:S(2)}) copy-start(bf16[8,64,256]{2,1,0:T(8,128)(2,1)S(1)} %all-to-all-done.a_ref) | copy-start | bytes 786436
  112.1 28.1 %collective-permute-start.18 = (bf16[4096,128]{1,0:T(8,128)(2,1)}, bf16[4096,128]{1,0:T(8,128)(2,1)}, u32[]{:S(2)}, u32[]{:S(2)}) collective-permute-start(bf16[4096,128]{1,0:T(8,128)(2,1)} %slice.24), channel_id=1, source_target_pairs={{0,2},{2,4},{4,6},{6,8},{8,10},{10,12},{12,14},{14,0},{1,3},{3,5},... | collective-permute-start | bytes 3145736 | tf_op jit(solution)/shard_map/ppermute | solution.py:555
  112.1 28.1 %collective-permute-start.19 = (bf16[4096,128]{1,0:T(8,128)(2,1)}, bf16[4096,128]{1,0:T(8,128)(2,1)}, u32[]{:S(2)}, u32[]{:S(2)}) collective-permute-start(bf16[4096,128]{1,0:T(8,128)(2,1)} %slice.25), channel_id=1, source_target_pairs={{0,14},{2,0},{4,2},{6,4},{8,6},{10,8},{12,10},{14,12},{1,15},{3,1}... | collective-permute-start | bytes 3145736 | tf_op jit(solution)/shard_map/ppermute | solution.py:555
  114.9 1.8 copy-start.6
  115.9 0.8 copy-start
  123.2 17.0 %copy-start.1 = (bf16[512,512]{1,0:T(8,128)(2,1)S(1)}, bf16[512,512]{1,0:T(8,128)(2,1)}, u32[]{:S(2)}) copy-start(bf16[512,512]{1,0:T(8,128)(2,1)} %copy-done) | copy-start | bytes 1572868
  123.2 17.0 %all-to-all-start.1 = ((bf16[16,160,128]{2,1,0:T(8,128)(2,1)}), bf16[16,160,128]{2,1,0:T(8,128)(2,1)S(1)}, u32[]{:S(2)}, u32[]{:S(2)}) async-start(bf16[16,160,128]{2,1,0:T(8,128)(2,1)} %get-tuple-element.64), calls=%async_computation.1 | async-start | bytes 1310720 | tf_op jit(solution)/shard_map/all_to_all | solution.py:648
  130.3 18.5 %collective-permute-start.22 = (bf16[2048,128]{1,0:T(8,128)(2,1)}, bf16[2048,128]{1,0:T(8,128)(2,1)}, u32[]{:S(2)}, u32[]{:S(2)}) collective-permute-start(bf16[2048,128]{1,0:T(8,128)(2,1)} %slice.27), channel_id=1, source_target_pairs={{0,2},{2,4},{4,6},{6,8},{8,10},{10,12},{12,14},{14,0},{1,3},{3,5},... | collective-permute-start | bytes 1572872 | tf_op jit(solution)/shard_map/ppermute | solution.py:555
  132.1 17.7 %collective-permute-start.21 = (bf16[2048,128]{1,0:T(8,128)(2,1)}, bf16[2048,128]{1,0:T(8,128)(2,1)S(1)}, u32[]{:S(2)}, u32[]{:S(2)}) collective-permute-start(bf16[2048,128]{1,0:T(8,128)(2,1)} %slice.26), channel_id=1, source_target_pairs={{0,14},{2,0},{4,2},{6,4},{8,6},{10,8},{12,10},{14,12},{1,15},{3,1}... | collective-permute-start | bytes 1572872 | tf_op jit(solution)/shard_map/ppermute | solution.py:555
  140.6 12.0 %copy-start.2 = (bf16[3,2048,128]{2,1,0:T(8,128)(2,1)S(1)}, bf16[3,2048,128]{2,1,0:T(8,128)(2,1)}, u32[]{:S(2)}) copy-start(bf16[3,2048,128]{2,1,0:T(8,128)(2,1)} %bundle.1) | copy-start | bytes 4718596
  140.6 12.0 %collective-permute-start.20 = (bf16[160,2048]{1,0:T(8,128)(2,1)S(1)}, bf16[160,2048]{1,0:T(8,128)(2,1)S(1)}, u32[]{:S(2)}, u32[]{:S(2)}) collective-permute-start(bf16[160,2048]{1,0:T(8,128)(2,1)S(1)} %rows_in.1.own_ref), channel_id=1, source_target_pairs={{0,1},{1,0},{2,3},{3,2},{4,5},{5,4},{6,7},{7,6},{8,9},{9,8},{10,11... | collective-permute-start | bytes 1966088 | tf_op jit(solution)/shard_map/ppermute | solution.py:568
  144.9 20.9 %collective-permute-start.25 = (bf16[2048,128]{1,0:T(8,128)(2,1)S(1)}, bf16[2048,128]{1,0:T(8,128)(2,1)S(1)}, u32[]{:S(2)}, u32[]{:S(2)}) collective-permute-start(bf16[2048,128]{1,0:T(8,128)(2,1)S(1)} %slice.30), channel_id=1, source_target_pairs={{0,2},{2,4},{4,6},{6,8},{8,10},{10,12},{12,14},{14,0},{1,3},{3,5},... | collective-permute-start | bytes 1572872 | tf_op jit(solution)/shard_map/ppermute | solution.py:555
  146.0 19.7 %collective-permute-start.26 = (bf16[2048,128]{1,0:T(8,128)(2,1)S(1)}, bf16[2048,128]{1,0:T(8,128)(2,1)S(1)}, u32[]{:S(2)}, u32[]{:S(2)}) collective-permute-start(bf16[2048,128]{1,0:T(8,128)(2,1)S(1)} %slice.31), channel_id=1, source_target_pairs={{0,14},{2,0},{4,2},{6,4},{8,6},{10,8},{12,10},{14,12},{1,15},{3,1}... | collective-permute-start | bytes 1572872 | tf_op jit(solution)/shard_map/ppermute | solution.py:555
  149.8 16.0 %collective-permute-start.23 = (bf16[1024,128]{1,0:T(8,128)(2,1)S(1)}, bf16[1024,128]{1,0:T(8,128)(2,1)S(1)}, u32[]{:S(2)}, u32[]{:S(2)}) collective-permute-start(bf16[1024,128]{1,0:T(8,128)(2,1)S(1)} %slice.32), channel_id=1, source_target_pairs={{0,2},{2,4},{4,6},{6,8},{8,10},{10,12},{12,14},{14,0},{1,3},{3,5},... | collective-permute-start | bytes 786440 | tf_op jit(solution)/shard_map/ppermute | solution.py:555
  149.9 15.8 %collective-permute-start.24 = (bf16[1024,128]{1,0:T(8,128)(2,1)S(1)}, bf16[1024,128]{1,0:T(8,128)(2,1)S(1)}, u32[]{:S(2)}, u32[]{:S(2)}) collective-permute-start(bf16[1024,128]{1,0:T(8,128)(2,1)S(1)} %slice.33), channel_id=1, source_target_pairs={{0,14},{2,0},{4,2},{6,4},{8,6},{10,8},{12,10},{14,12},{1,15},{3,1}... | collective-permute-start | bytes 786440 | tf_op jit(solution)/shard_map/ppermute | solution.py:555
  168.2 3.3 %collective-permute-start.27 = (bf16[160,2048]{1,0:T(8,128)(2,1)S(1)}, bf16[160,2048]{1,0:T(8,128)(2,1)S(1)}, u32[]{:S(2)}, u32[]{:S(2)}) collective-permute-start(bf16[160,2048]{1,0:T(8,128)(2,1)S(1)} %get-tuple-element.69), channel_id=1, source_target_pairs={{0,1},{1,0},{2,3},{3,2},{4,5},{5,4},{6,7},{7,6},{8,9},{9,8},{10,11... | collective-permute-start | bytes 1966088 | tf_op jit(solution)/shard_map/ppermute | solution.py:568
  171.5 18.7 %copy-start.7 = (bf16[64,2048]{1,0:T(8,128)(2,1)S(1)}, bf16[64,2048]{1,0:T(8,128)(2,1)}, u32[]{:S(2)}) copy-start(bf16[64,2048]{1,0:T(8,128)(2,1)} %get-tuple-element.70.upd_ref) | copy-start | bytes 786436

commit v2 on v1

--- a/solution.py
+++ b/solution.py
@@ -634,7 +634,7 @@
     rest_p, rest_m, attended = lax.optimization_barrier((w2p[third:], w2m[third:], attended))
     w3p.append(shift(rest_p, "z", 1))
     w3m.append(shift(rest_m, "z", -1))
-    w4 = [shift(w3p[0][: third // 2], "z", 1), shift(w3m[0][third // 2 :], "z", -1)]
+    w4 = [shift(w3p[0], "z", 1)]
     updated, outgoing = project(
         attended,
         out_weight,
@@ -647,7 +647,9 @@
     )
     arrived = lax.all_to_all(outgoing, SP, 0, 0, tiled=True)
     rest_p, rest_m, arrived = lax.optimization_barrier((w3p[1], w3m[1], arrived))
-    w4 += [shift(rest_p[:third], "z", 1), shift(rest_m[third:], "z", -1)]
+    cut = 3 * third // 4
+    w4 += [shift(rest_m[cut:], "z", -1), shift(rest_p[:cut], "z", 1)]
+    w4 = [w4[0], w4[2], w4[1]]
     rows = rows_in(arrived, swap)
     sib_rows = swap_cores(rows)
     (acc,) = expert(rows, sib_rows, [[w0], [w1p], [w1m], [w2p], [w2m], w3p], None, False)

time: 192 us -> 196 us (1.021)
  waiting for transfers between devices: 31.3 us -> 46.5 us
  starting transfers between devices: 62.8 us -> 55.6 us
  local copies, waits for them, and re-layouts: 13.8 us -> 11 us
    ppermute x22 -> x21, waiting for transfers between devices: 14.6 us -> 25.3 us  [shift(): lax.ppermute(value, axis, [(i, (i + by) % size) for i in range(size)])]
    ppermute x22 -> x21, starting transfers between devices: 38.6 us -> 32 us  [shift(): lax.ppermute(value, axis, [(i, (i + by) % size) for i in range(size)])]
    all_to_all x1, waiting for transfers between devices: 5.43 us -> 10 us  [local(): arrived = lax.all_to_all(outgoing, SP, 0, 0, tiled=True)]
    slice x4 -> x2, local copies, waits for them, and re-layouts: 3.14 us -> 1.06 us  [local(): w4 += [shift(rest_m[cut:], 'z', -1), shift(rest_p[:cut], 'z', 1)]]
  transfers between devices with their start and end apart: 30 -> 29, of which waited for: 10 -> 11; matrix products, arithmetic and copies ran while one was open for 6% -> 4% of each run, Pallas kernels for 30% -> 30%
where the time goes in v2:
time: 196 us; the launch traced here: 195 us
  Pallas kernels  63.7 us (32%)
  starting transfers between devices  55.6 us (28%)
  waiting for transfers between devices  46.5 us (24%)
  blocking collectives  16.7 us (9%)
  local copies, waits for them, and re-layouts  11 us (6%)
    pallas_call x3, Pallas kernels, attend(): pl.pallas_call(functools.partial(attend_kernel, first, last, count), grid...  35.6 us
    ppermute x21, starting transfers between devices, shift(): lax.ppermute(value, axis, [(i, (i + by) % size) for i in range(size)])  32 us
    ppermute x21, waiting for transfers between devices, shift(): lax.ppermute(value, axis, [(i, (i + by) % size) for i in range(size)])  25.3 us
    all_to_all x1, blocking collectives, local(): returned = lax.all_to_all(result, SP, 0, 0, tiled=True)  16.7 us
    all_to_all x1, waiting for transfers between devices, local(): arrived = lax.all_to_all(outgoing, SP, 0, 0, tiled=True)  10 us
    ppermute x4, starting transfers between devices, swap_cores(): return lax.ppermute(value, 'core', ((0, 1), (1, 0)))  9.89 us
    all_to_all x1, waiting for transfers between devices, local(): attended = lax.all_to_all(merged, 'z', 0, 0, tiled=True)  7.69 us
    pallas_call x2, Pallas kernels, expert(): pl.pallas_call(functools.partial(expert_kernel, tuple((len(piece) for pie...  7.27 us
  transfers between devices with their start and end apart: 29, of which 11 were waited for; matrix products, arithmetic and copies ran while one was open for 4% of the time, Pallas kernels for 30%

profile of v2, /device:TPU:1, one launch (start us, length us, event | category | flops | bytes accessed | tf_op | source)
XLA Modules:
  0.0 195.4 jit_solution(8654383775781929265)
XLA Ops:
  0.0 2.4 %bundle.1 = bf16[3,2048,128]{2,1,0:T(8,128)(2,1)} custom-call(bf16[2048,128]{1,0:T(8,128)(2,1)} %bitcast.16, bf16[2048,128]{1,0:T(8,128)(2,1)} %bitcast.17, bf16[128,2048]{1,0:T(8,128)(2,1)} %bitcast.18), custom_call_target="tpu_custom_call" | custom-call | tf_op jit(solution)/shard_map/bundle/pallas_call | solution.py:43
  2.4 2.5 %collective-permute-start = (bf16[6144,128]{1,0:T(8,128)(2,1)}, bf16[6144,128]{1,0:T(8,128)(2,1)}, u32[]{:S(2)}, u32[]{:S(2)}) collective-permute-start(bf16[6144,128]{1,0:T(8,128)(2,1)} %bitcast.11), channel_id=1, source_target_pairs={{0,2},{2,4},{4,6},{6,8},{8,10},{10,12},{12,14},{14,0},{1,3},{3,5},... | collective-permute-start | bytes 4718600 | tf_op jit(solution)/shard_map/ppermute | solution.py:555
  4.8 3.9 %collective-permute-start.1 = (bf16[6144,128]{1,0:T(8,128)(2,1)}, bf16[6144,128]{1,0:T(8,128)(2,1)}, u32[]{:S(2)}, u32[]{:S(2)}) collective-permute-start(bf16[6144,128]{1,0:T(8,128)(2,1)} %bitcast.12), channel_id=1, source_target_pairs={{0,14},{2,0},{4,2},{6,4},{8,6},{10,8},{12,10},{14,12},{1,15},{3,1}... | collective-permute-start | bytes 4718600 | tf_op jit(solution)/shard_map/ppermute | solution.py:555
  8.8 0.6 pad_add_fusion.where_ref
  9.4 0.9 fusion
  10.3 5.3 %prep.1 = (bf16[1024,128]{1,0:T(8,128)(2,1)}, bf16[256,256]{1,0:T(8,128)(2,1)}, bf16[256,256]{1,0:T(8,128)(2,1)}) custom-call(s32[2]{0:T(128)} %pad_add_fusion.where_ref, bf16[1024,128]{1,0:T(8,128)(2,1)} %q_ref.1, bf16[1024,512]{1,0:T(8,128)(2,1)} %k_ref.1, bf16[1024,512]{1,0:T(8,128)(2,1)} %v_ref.1, f32[1,128]{1,0:T(1,128)} %bitcast.20, ...), custom_call_target="tpu_custom_call" | custom-call | tf_op jit(solution)/shard_map/prep/pallas_call | solution.py:95
  15.5 1.2 collective-permute-start.3
  16.7 1.5 collective-permute-start.4
  18.2 1.5 collective-permute-start.5
  19.7 1.4 collective-permute-done.3.refs_1_
  21.2 1.3 collective-permute-start.6
  22.5 1.4 collective-permute-start.7
  23.9 1.2 collective-permute-done.5.refs_3_
  25.1 2.9 %collective-permute-start.8 = (bf16[256,256]{1,0:T(8,128)(2,1)}, bf16[256,256]{1,0:T(8,128)(2,1)S(1)}, u32[]{:S(2)}, u32[]{:S(2)}) collective-permute-start(bf16[256,256]{1,0:T(8,128)(2,1)} %get-tuple-element.41.refs_4_), channel_id=1, source_target_pairs={{0,128},{64,192},{128,0},{192,64},{1,129},{65,193},{129,1},{193,65... | collective-permute-start | bytes 393224 | tf_op jit(solution)/shard_map/ppermute | solution.py:555
  28.1 3.2 %collective-permute-done.8.refs_7_ = bf16[256,256]{1,0:T(8,128)(2,1)S(1)} collective-permute-done((bf16[256,256]{1,0:T(8,128)(2,1)}, bf16[256,256]{1,0:T(8,128)(2,1)S(1)}, u32[]{:S(2)}, u32[]{:S(2)}) %collective-permute-start.8) | collective-permute-done | bytes 131104 | tf_op jit(solution)/shard_map/ppermute | solution.py:555
  31.2 0.9 copy-done.8
  32.1 0.9 copy-done.9
  33.1 2.4 %collective-permute-start.10 = (bf16[1024,256]{1,0:T(8,128)(2,1)S(1)}, bf16[1024,256]{1,0:T(8,128)(2,1)S(1)}, u32[]{:S(2)}, u32[]{:S(2)}) collective-permute-start(bf16[1024,256]{1,0:T(8,128)(2,1)S(1)} %get-tuple-element.42.refs_0_), channel_id=1, source_target_pairs={{0,192},{64,0},{128,64},{192,128},{1,193},{65,1},{129,65},{193,129... | collective-permute-start | bytes 1572872 | tf_op jit(solution)/shard_map/ppermute | solution.py:555
  35.5 3.1 %collective-permute-start.2 = (bf16[1024,128]{1,0:T(8,128)(2,1)}, bf16[1024,128]{1,0:T(8,128)(2,1)S(1)}, u32[]{:S(2)}, u32[]{:S(2)}) collective-permute-start(bf16[1024,128]{1,0:T(8,128)(2,1)} %get-tuple-element.39.own_ref), channel_id=1, source_target_pairs={{0,1},{1,0},{2,3},{3,2},{4,5},{5,4},{6,7},{7,6},{8,9},{9,8},{10,11... | collective-permute-start | bytes 786440 | tf_op jit(solution)/shard_map/ppermute | solution.py:568
  38.6 1.1 collective-permute-start.11
  39.7 0.2 collective-permute-done.2.sib_ref
  40.0 2.9 %collective-permute-start.12 = (bf16[1024,256]{1,0:T(8,128)(2,1)S(1)}, bf16[1024,256]{1,0:T(8,128)(2,1)S(1)}, u32[]{:S(2)}, u32[]{:S(2)}) collective-permute-start(bf16[1024,256]{1,0:T(8,128)(2,1)S(1)} %get-tuple-element.43.refs_1_), channel_id=1, source_target_pairs={{0,48},{16,0},{32,16},{48,32},{1,49},{17,1},{33,17},{49,33},{2,50}... | collective-permute-start | bytes 1572872 | tf_op jit(solution)/shard_map/ppermute | solution.py:555
  42.9 1.7 collective-permute-done.10.refs_1_
  44.5 2.3 %collective-permute-start.9 = (bf16[1024,256]{1,0:T(8,128)(2,1)S(1)}, bf16[1024,256]{1,0:T(8,128)(2,1)S(1)}, u32[]{:S(2)}, u32[]{:S(2)}) collective-permute-start(bf16[1024,256]{1,0:T(8,128)(2,1)S(1)} %get-tuple-element.42.refs_0_), channel_id=1, source_target_pairs={{0,64},{64,128},{128,192},{192,0},{1,65},{65,129},{129,193},{193,1... | collective-permute-start | bytes 1572872 | tf_op jit(solution)/shard_map/ppermute | solution.py:555
  46.9 0.9 copy-done.3
  47.8 10.1 %attend.3 = (f32[2,1024,256]{2,1,0:T(8,128)S(1)}, f32[2,1024,128]{2,1,0:T(8,128)S(1)}) custom-call(s32[2]{0:T(128)S(1)} %copy-done.10, bf16[1024,128]{1,0:T(8,128)(2,1)S(1)} %copy-done.3, bf16[1024,128]{1,0:T(8,128)(2,1)S(1)} %collective-permute-done.2.sib_ref, bf16[1024,256]{1,0:T(8,128)(2,1)S(1)} %get-tuple-element.42.refs_0_, ...), custom_call_target="tpu_custom_call" | custom-call | tf_op jit(solution)/shard_map/attend/pallas_call | solution.py:228
  58.1 0.7 copy-done.4
  58.8 2.7 %collective-permute-start.14 = (bf16[6144,128]{1,0:T(8,128)(2,1)}, bf16[6144,128]{1,0:T(8,128)(2,1)}, u32[]{:S(2)}, u32[]{:S(2)}) collective-permute-start(bf16[6144,128]{1,0:T(8,128)(2,1)} %collective-permute-done.1.refs_2_), channel_id=1, source_target_pairs={{0,14},{2,0},{4,2},{6,4},{8,6},{10,8},{12,10},{14,12},{1,15},{3,1}... | collective-permute-start | bytes 4718600 | tf_op jit(solution)/shard_map/ppermute | solution.py:555
  61.5 2.4 %collective-permute-start.15 = (bf16[1024,256]{1,0:T(8,128)(2,1)S(1)}, bf16[1024,256]{1,0:T(8,128)(2,1)S(1)}, u32[]{:S(2)}, u32[]{:S(2)}) collective-permute-start(bf16[1024,256]{1,0:T(8,128)(2,1)S(1)} %broadcast_select_fusion.1), channel_id=1, source_target_pairs={{0,64},{1,193},{64,128},{65,1},{128,192},{129,65},{192,0},{193,129... | collective-permute-start | bytes 1572872 | tf_op jit(solution)/shard_map/ppermute | solution.py:564
  64.0 15.1 %attend.4 = (f32[2,1024,256]{2,1,0:T(8,128)S(1)}, f32[2,1024,128]{2,1,0:T(8,128)S(1)}) custom-call(s32[2]{0:T(128)S(1)} %copy-done.10, bf16[1024,128]{1,0:T(8,128)(2,1)S(1)} %copy-done.3, bf16[1024,128]{1,0:T(8,128)(2,1)S(1)} %collective-permute-done.2.sib_ref, bf16[1024,256]{1,0:T(8,128)(2,1)S(1)} %collective-permute-done.9.refs_0_, ...), custom_call_target="tpu_custom_call" | custom-call | tf_op jit(solution)/shard_map/attend/pallas_call | solution.py:228
  79.1 10.3 %attend.5 = (f32[2,8,64,256]{3,2,1,0:T(8,128)S(1)}, bf16[2,8,64,256]{3,2,1,0:T(8,128)(2,1)S(1)}) custom-call(s32[2]{0:T(128)S(1)} %copy-done.10, bf16[1024,128]{1,0:T(8,128)(2,1)S(1)} %copy-done.3, bf16[1024,128]{1,0:T(8,128)(2,1)S(1)} %collective-permute-done.2.sib_ref, bf16[1024,256]{1,0:T(8,128)(2,1)S(1)} %collective-permute-done.15.refs_0_, ...), custom_call_target="tpu_custom_call" | custom-call | tf_op jit(solution)/shard_map/attend/pallas_call | solution.py:228
  89.5 2.6 %collective-permute-start.17 = (bf16[2,8,64,256]{3,2,1,0:T(8,128)(2,1)S(1)}, bf16[2,8,64,256]{3,2,1,0:T(8,128)(2,1)S(1)}, u32[]{:S(2)}, u32[]{:S(2)}) collective-permute-start(bf16[2,8,64,256]{3,2,1,0:T(8,128)(2,1)S(1)} %get-tuple-element.59), channel_id=1, source_target_pairs={{0,1},{1,0},{2,3},{3,2},{4,5},{5,4},{6,7},{7,6},{8,9},{9,8},{10,11... | collective-permute-start | bytes 1572872 | tf_op jit(solution)/shard_map/ppermute | solution.py:568
  92.1 1.5 collective-permute-done.17.got_ref
  93.6 2.3 %merge.1 = bf16[8,64,256]{2,1,0:T(8,128)(2,1)} custom-call(s32[2]{0:T(128)S(1)} %copy-done.10, f32[2,8,64,256]{3,2,1,0:T(8,128)S(1)} %get-tuple-element.56.keep_ref, bf16[2,8,64,256]{3,2,1,0:T(8,128)(2,1)S(1)} %collective-permute-done.17.got_ref), custom_call_target="tpu_custom_call" | custom-call | tf_op jit(solution)/shard_map/merge/pallas_call | solution.py:268
  95.9 5.1 %all-to-all-start = ((bf16[8,64,256]{2,1,0:T(8,128)(2,1)}), bf16[8,64,256]{2,1,0:T(8,128)(2,1)S(1)}, u32[]{:S(2)}, u32[]{:S(2)}) async-start(bf16[8,64,256]{2,1,0:T(8,128)(2,1)} %merge.1), calls=%async_computation | async-start | bytes 524288 | tf_op jit(solution)/shard_map/all_to_all | solution.py:633
  101.0 1.0 slice.18
  102.0 2.4 %slice.19 = bf16[4096,128]{1,0:T(8,128)(2,1)} slice(bf16[6144,128]{1,0:T(8,128)(2,1)} %collective-permute-done.14.refs_4_), slice={[2048:6144], [0:128]} | slice | bytes 2097152 | tf_op jit(solution)/shard_map/slice | solution.py:634
  104.4 7.7 %all-to-all-done.a_ref = bf16[8,64,256]{2,1,0:T(8,128)(2,1)S(1)} async-done(((bf16[8,64,256]{2,1,0:T(8,128)(2,1)}), bf16[8,64,256]{2,1,0:T(8,128)(2,1)S(1)}, u32[]{:S(2)}, u32[]{:S(2)}) %all-to-all-start) | async-done | bytes 262176 | tf_op jit(solution)/shard_map/all_to_all | solution.py:633
  112.1 2.7 %collective-permute-start.19 = (bf16[4096,128]{1,0:T(8,128)(2,1)}, bf16[4096,128]{1,0:T(8,128)(2,1)S(1)}, u32[]{:S(2)}, u32[]{:S(2)}) collective-permute-start(bf16[4096,128]{1,0:T(8,128)(2,1)} %slice.19), channel_id=1, source_target_pairs={{0,14},{2,0},{4,2},{6,4},{8,6},{10,8},{12,10},{14,12},{1,15},{3,1}... | collective-permute-start | bytes 3145736 | tf_op jit(solution)/shard_map/ppermute | solution.py:555
  114.8 0.1 copy.18.route_ref
  114.9 0.1 copy.16.score_ref
  115.0 0.1 copy.17.prob_ref
  115.1 0.7 plan.1
  115.8 0.8 copy-done
  116.7 6.6 %project.1 = (bf16[64,2048]{1,0:T(8,128)(2,1)}, bf16[16,160,128]{2,1,0:T(8,128)(2,1)}) custom-call(bf16[8,64,256]{2,1,0:T(8,128)(2,1)} %copy-done.12, bf16[2048,2048]{1,0:T(8,128)(2,1)} %w_ref.1, bf16[64,2048]{1,0:T(8,128)(2,1)} %res_ref.1, f32[1,2048]{1,0:T(1,128)} %bitcast.19, s32[64,2]{1,0:T(8,128)} %copy-done.6, s32[2,64]{1,0:T(2,128)} %bitcast.14, ...), custom_call_target="tpu_custom_call" | custom-call | tf_op jit(solution)/shard_map/project/pallas_call | solution.py:363
  123.2 6.2 %all-to-all-start.1 = ((bf16[16,160,128]{2,1,0:T(8,128)(2,1)}), bf16[16,160,128]{2,1,0:T(8,128)(2,1)}, u32[]{:S(2)}, u32[]{:S(2)}) async-start(bf16[16,160,128]{2,1,0:T(8,128)(2,1)} %get-tuple-element.64), calls=%async_computation.1 | async-start | bytes 1310720 | tf_op jit(solution)/shard_map/all_to_all | solution.py:648
  129.4 0.9 slice.21
  130.3 10.0 %all-to-all-done.1.in_ref = bf16[16,160,128]{2,1,0:T(8,128)(2,1)} async-done(((bf16[16,160,128]{2,1,0:T(8,128)(2,1)}), bf16[16,160,128]{2,1,0:T(8,128)(2,1)}, u32[]{:S(2)}, u32[]{:S(2)}) %all-to-all-start.1) | async-done | bytes 655392 | tf_op jit(solution)/shard_map/all_to_all | solution.py:648
  140.3 1.5 rows_in.1.own_ref
  141.9 3.2 %collective-permute-start.20 = (bf16[160,2048]{1,0:T(8,128)(2,1)S(1)}, bf16[160,2048]{1,0:T(8,128)(2,1)S(1)}, u32[]{:S(2)}, u32[]{:S(2)}) collective-permute-start(bf16[160,2048]{1,0:T(8,128)(2,1)S(1)} %rows_in.1.own_ref), channel_id=1, source_target_pairs={{0,1},{1,0},{2,3},{3,2},{4,5},{5,4},{6,7},{7,6},{8,9},{9,8},{10,11... | collective-permute-start | bytes 1966088 | tf_op jit(solution)/shard_map/ppermute | solution.py:568
  145.1 0.1 collective-permute-start.25
  145.2 1.1 slice.20
  146.3 0.1 collective-permute-start.21
  146.4 1.5 collective-permute-done.22.refs_5_
  147.9 1.0 slice.22
  148.9 1.4 collective-permute-start.24
  150.4 6.0 %expert.2.refs_5_ = f32[320,2048]{1,0:T(8,128)S(1)} custom-call(bf16[160,2048]{1,0:T(8,128)(2,1)S(1)} %rows_in.1.own_ref, bf16[160,2048]{1,0:T(8,128)(2,1)S(1)} %collective-permute-done.20.sib_ref, bf16[6144,128]{1,0:T(8,128)(2,1)S(1)} %bitcast.13, bf16[6144,128]{1,0:T(8,128)(2,1)} %collective-permute-done.refs_1_, ...), custom_call_target="tpu_custom_call" | custom-call | tf_op jit(solution)/shard_map/expert/pallas_call | solution.py:459
  156.4 16.3 %collective-permute-done.21.refs_0_ = bf16[2048,128]{1,0:T(8,128)(2,1)S(1)} collective-permute-done((bf16[2048,128]{1,0:T(8,128)(2,1)S(1)}, bf16[2048,128]{1,0:T(8,128)(2,1)S(1)}, u32[]{:S(2)}, u32[]{:S(2)}) %collective-permute-start.21) | collective-permute-done | bytes 524320 | tf_op jit(solution)/shard_map/ppermute | solution.py:555
  172.7 1.3 expert.3
  174.0 1.0 collective-permute-start.26
  174.9 1.7 collective-permute-done.26.got_ref
  176.7 0.4 finish.1
  177.1 16.7 %all_to_all.15.in_ref = bf16[16,160,128]{2,1,0:T(8,128)(2,1)S(1)} all-to-all(bf16[16,160,128]{2,1,0:T(8,128)(2,1)S(1)} %finish.1), channel_id=1, replica_groups=mesh['y'=4,'x'=4,'z'=8,'core'=2] {'y','x'}, dimensions={0} | all-to-all | bytes 1310720 | tf_op jit(solution)/shard_map/all_to_all | solution.py:658
  193.8 1.6 mix.1
  (54 shorter events, 0.4 us)
Async XLA Ops:
  2.4 55.6 %collective-permute-start = (bf16[6144,128]{1,0:T(8,128)(2,1)}, bf16[6144,128]{1,0:T(8,128)(2,1)}, u32[]{:S(2)}, u32[]{:S(2)}) collective-permute-start(bf16[6144,128]{1,0:T(8,128)(2,1)} %bitcast.11), channel_id=1, source_target_pairs={{0,2},{2,4},{4,6},{6,8},{8,10},{10,12},{12,14},{14,0},{1,3},{3,5},... | collective-permute-start | bytes 4718600 | tf_op jit(solution)/shard_map/ppermute | solution.py:555
  4.8 53.2 %collective-permute-start.1 = (bf16[6144,128]{1,0:T(8,128)(2,1)}, bf16[6144,128]{1,0:T(8,128)(2,1)}, u32[]{:S(2)}, u32[]{:S(2)}) collective-permute-start(bf16[6144,128]{1,0:T(8,128)(2,1)} %bitcast.12), channel_id=1, source_target_pairs={{0,14},{2,0},{4,2},{6,4},{8,6},{10,8},{12,10},{14,12},{1,15},{3,1}... | collective-permute-start | bytes 4718600 | tf_op jit(solution)/shard_map/ppermute | solution.py:555
  10.3 36.6 %copy-start.10 = (s32[2]{0:T(128)S(1)}, s32[2]{0:T(128)}, u32[]{:S(2)}) copy-start(s32[2]{0:T(128)} %pad_add_fusion.where_ref) | copy-start | bytes 28
  15.5 5.6 %collective-permute-start.3 = (bf16[256,256]{1,0:T(8,128)(2,1)}, bf16[256,256]{1,0:T(8,128)(2,1)S(1)}, u32[]{:S(2)}, u32[]{:S(2)}) collective-permute-start(bf16[256,256]{1,0:T(8,128)(2,1)} %get-tuple-element.40.refs_0_), channel_id=1, source_target_pairs={{0,16},{16,32},{32,48},{48,0},{1,17},{17,33},{33,49},{49,1},{2,18}... | collective-permute-start | bytes 393224 | tf_op jit(solution)/shard_map/ppermute | solution.py:555
  16.7 5.7 %collective-permute-start.4 = (bf16[256,256]{1,0:T(8,128)(2,1)}, bf16[256,256]{1,0:T(8,128)(2,1)S(1)}, u32[]{:S(2)}, u32[]{:S(2)}) collective-permute-start(bf16[256,256]{1,0:T(8,128)(2,1)} %get-tuple-element.40.refs_0_), channel_id=1, source_target_pairs={{0,48},{16,0},{32,16},{48,32},{1,49},{17,1},{33,17},{49,33},{2,50}... | collective-permute-start | bytes 393224 | tf_op jit(solution)/shard_map/ppermute | solution.py:555
  18.2 6.9 %collective-permute-start.5 = (bf16[256,256]{1,0:T(8,128)(2,1)}, bf16[256,256]{1,0:T(8,128)(2,1)S(1)}, u32[]{:S(2)}, u32[]{:S(2)}) collective-permute-start(bf16[256,256]{1,0:T(8,128)(2,1)} %get-tuple-element.40.refs_0_), channel_id=1, source_target_pairs={{0,32},{16,48},{32,0},{48,16},{1,33},{17,49},{33,1},{49,17},{2,34}... | collective-permute-start | bytes 393224 | tf_op jit(solution)/shard_map/ppermute | solution.py:555
  21.2 6.9 %collective-permute-start.6 = (bf16[256,256]{1,0:T(8,128)(2,1)}, bf16[256,256]{1,0:T(8,128)(2,1)S(1)}, u32[]{:S(2)}, u32[]{:S(2)}) collective-permute-start(bf16[256,256]{1,0:T(8,128)(2,1)} %get-tuple-element.41.refs_4_), channel_id=1, source_target_pairs={{0,64},{64,128},{128,192},{192,0},{1,65},{65,129},{129,193},{193,1... | collective-permute-start | bytes 393224 | tf_op jit(solution)/shard_map/ppermute | solution.py:555
  22.5 5.6 %collective-permute-start.7 = (bf16[256,256]{1,0:T(8,128)(2,1)}, bf16[256,256]{1,0:T(8,128)(2,1)S(1)}, u32[]{:S(2)}, u32[]{:S(2)}) collective-permute-start(bf16[256,256]{1,0:T(8,128)(2,1)} %get-tuple-element.41.refs_4_), channel_id=1, source_target_pairs={{0,192},{64,0},{128,64},{192,128},{1,193},{65,1},{129,65},{193,129... | collective-permute-start | bytes 393224 | tf_op jit(solution)/shard_map/ppermute | solution.py:555
  25.1 6.1 %collective-permute-start.8 = (bf16[256,256]{1,0:T(8,128)(2,1)}, bf16[256,256]{1,0:T(8,128)(2,1)S(1)}, u32[]{:S(2)}, u32[]{:S(2)}) collective-permute-start(bf16[256,256]{1,0:T(8,128)(2,1)} %get-tuple-element.41.refs_4_), channel_id=1, source_target_pairs={{0,128},{64,192},{128,0},{192,64},{1,129},{65,193},{129,1},{193,65... | collective-permute-start | bytes 393224 | tf_op jit(solution)/shard_map/ppermute | solution.py:555
  31.2 0.9 copy-start.8
  32.1 0.9 copy-start.9
  33.1 11.4 %collective-permute-start.10 = (bf16[1024,256]{1,0:T(8,128)(2,1)S(1)}, bf16[1024,256]{1,0:T(8,128)(2,1)S(1)}, u32[]{:S(2)}, u32[]{:S(2)}) collective-permute-start(bf16[1024,256]{1,0:T(8,128)(2,1)S(1)} %get-tuple-element.42.refs_0_), channel_id=1, source_target_pairs={{0,192},{64,0},{128,64},{192,128},{1,193},{65,1},{129,65},{193,129... | collective-permute-start | bytes 1572872 | tf_op jit(solution)/shard_map/ppermute | solution.py:555
  35.5 4.5 %collective-permute-start.2 = (bf16[1024,128]{1,0:T(8,128)(2,1)}, bf16[1024,128]{1,0:T(8,128)(2,1)S(1)}, u32[]{:S(2)}, u32[]{:S(2)}) collective-permute-start(bf16[1024,128]{1,0:T(8,128)(2,1)} %get-tuple-element.39.own_ref), channel_id=1, source_target_pairs={{0,1},{1,0},{2,3},{3,2},{4,5},{5,4},{6,7},{7,6},{8,9},{9,8},{10,11... | collective-permute-start | bytes 786440 | tf_op jit(solution)/shard_map/ppermute | solution.py:568
  38.6 19.4 %collective-permute-start.11 = (bf16[1024,256]{1,0:T(8,128)(2,1)S(1)}, bf16[1024,256]{1,0:T(8,128)(2,1)S(1)}, u32[]{:S(2)}, u32[]{:S(2)}) collective-permute-start(bf16[1024,256]{1,0:T(8,128)(2,1)S(1)} %get-tuple-element.43.refs_1_), channel_id=1, source_target_pairs={{0,16},{16,32},{32,48},{48,0},{1,17},{17,33},{33,49},{49,1},{2,18}... | collective-permute-start | bytes 1572872 | tf_op jit(solution)/shard_map/ppermute | solution.py:555
  40.0 18.0 %collective-permute-start.12 = (bf16[1024,256]{1,0:T(8,128)(2,1)S(1)}, bf16[1024,256]{1,0:T(8,128)(2,1)S(1)}, u32[]{:S(2)}, u32[]{:S(2)}) collective-permute-start(bf16[1024,256]{1,0:T(8,128)(2,1)S(1)} %get-tuple-element.43.refs_1_), channel_id=1, source_target_pairs={{0,48},{16,0},{32,16},{48,32},{1,49},{17,1},{33,17},{49,33},{2,50}... | collective-permute-start | bytes 1572872 | tf_op jit(solution)/shard_map/ppermute | solution.py:555
  44.5 13.4 %collective-permute-start.9 = (bf16[1024,256]{1,0:T(8,128)(2,1)S(1)}, bf16[1024,256]{1,0:T(8,128)(2,1)S(1)}, u32[]{:S(2)}, u32[]{:S(2)}) collective-permute-start(bf16[1024,256]{1,0:T(8,128)(2,1)S(1)} %get-tuple-element.42.refs_0_), channel_id=1, source_target_pairs={{0,64},{64,128},{128,192},{192,0},{1,65},{65,129},{129,193},{193,1... | collective-permute-start | bytes 1572872 | tf_op jit(solution)/shard_map/ppermute | solution.py:555
  46.9 1.0 copy-start.3
  58.0 0.8 copy-start.4
  58.8 20.3 %collective-permute-start.16 = (bf16[1024,256]{1,0:T(8,128)(2,1)S(1)}, bf16[1024,256]{1,0:T(8,128)(2,1)S(1)}, u32[]{:S(2)}, u32[]{:S(2)}) collective-permute-start(bf16[1024,256]{1,0:T(8,128)(2,1)S(1)} %broadcast_select_fusion), channel_id=1, source_target_pairs={{0,16},{1,49},{16,32},{17,1},{32,48},{33,17},{48,0},{49,33},{2,18}... | collective-permute-start | bytes 1572872 | tf_op jit(solution)/shard_map/ppermute | solution.py:564
  58.8 5.2 %copy-start.5 = (bf16[1024,256]{1,0:T(8,128)(2,1)S(1)}, bf16[1024,256]{1,0:T(8,128)(2,1)}, u32[]{:S(2)}) copy-start(bf16[1024,256]{1,0:T(8,128)(2,1)} %copy-done.4) | copy-start | bytes 1572868
  58.8 42.2 %collective-permute-start.13 = (bf16[6144,128]{1,0:T(8,128)(2,1)}, bf16[6144,128]{1,0:T(8,128)(2,1)S(1)}, u32[]{:S(2)}, u32[]{:S(2)}) collective-permute-start(bf16[6144,128]{1,0:T(8,128)(2,1)} %collective-permute-done.refs_1_), channel_id=1, source_target_pairs={{0,2},{2,4},{4,6},{6,8},{8,10},{10,12},{12,14},{14,0},{1,3},{3,5},... | collective-permute-start | bytes 4718600 | tf_op jit(solution)/shard_map/ppermute | solution.py:555
  58.8 42.2 %collective-permute-start.14 = (bf16[6144,128]{1,0:T(8,128)(2,1)}, bf16[6144,128]{1,0:T(8,128)(2,1)}, u32[]{:S(2)}, u32[]{:S(2)}) collective-permute-start(bf16[6144,128]{1,0:T(8,128)(2,1)} %collective-permute-done.1.refs_2_), channel_id=1, source_target_pairs={{0,14},{2,0},{4,2},{6,4},{8,6},{10,8},{12,10},{14,12},{1,15},{3,1}... | collective-permute-start | bytes 4718600 | tf_op jit(solution)/shard_map/ppermute | solution.py:555
  61.5 17.6 %collective-permute-start.15 = (bf16[1024,256]{1,0:T(8,128)(2,1)S(1)}, bf16[1024,256]{1,0:T(8,128)(2,1)S(1)}, u32[]{:S(2)}, u32[]{:S(2)}) collective-permute-start(bf16[1024,256]{1,0:T(8,128)(2,1)S(1)} %broadcast_select_fusion.1), channel_id=1, source_target_pairs={{0,64},{1,193},{64,128},{65,1},{128,192},{129,65},{192,0},{193,129... | collective-permute-start | bytes 1572872 | tf_op jit(solution)/shard_map/ppermute | solution.py:564
  89.5 4.1 %collective-permute-start.17 = (bf16[2,8,64,256]{3,2,1,0:T(8,128)(2,1)S(1)}, bf16[2,8,64,256]{3,2,1,0:T(8,128)(2,1)S(1)}, u32[]{:S(2)}, u32[]{:S(2)}) collective-permute-start(bf16[2,8,64,256]{3,2,1,0:T(8,128)(2,1)S(1)} %get-tuple-element.59), channel_id=1, source_target_pairs={{0,1},{1,0},{2,3},{3,2},{4,5},{5,4},{6,7},{7,6},{8,9},{9,8},{10,11... | collective-permute-start | bytes 1572872 | tf_op jit(solution)/shard_map/ppermute | solution.py:568
  95.9 16.2 %all-to-all-start = ((bf16[8,64,256]{2,1,0:T(8,128)(2,1)}), bf16[8,64,256]{2,1,0:T(8,128)(2,1)S(1)}, u32[]{:S(2)}, u32[]{:S(2)}) async-start(bf16[8,64,256]{2,1,0:T(8,128)(2,1)} %merge.1), calls=%async_computation | async-start | bytes 524288 | tf_op jit(solution)/shard_map/all_to_all | solution.py:633
  102.0 12.7 %copy-start.11 = (s32[64,2]{0,1:T(2,128)S(1)}, s32[64,2]{0,1:T(2,128)}, u32[]{:S(2)}) copy-start(s32[64,2]{0,1:T(2,128)} %param.22) | copy-start | bytes 1540
  102.0 12.8 %copy-start.13 = (f32[64,2]{0,1:T(2,128)S(1)}, f32[64,2]{0,1:T(2,128)}, u32[]{:S(2)}) copy-start(f32[64,2]{0,1:T(2,128)} %param.23) | copy-start | bytes 1540
  102.0 12.9 %copy-start.14 = (f32[64]{0:T(128)S(1)}, f32[64]{0:T(128)}, u32[]{:S(2)}) copy-start(f32[64]{0:T(128)} %param.24) | copy-start | bytes 772
  112.1 4.5 %copy-start.12 = (bf16[8,64,256]{2,1,0:T(8,128)(2,1)}, bf16[8,64,256]{2,1,0:T(8,128)(2,1)S(1)}, u32[]{:S(2)}) copy-start(bf16[8,64,256]{2,1,0:T(8,128)(2,1)S(1)} %all-to-all-done.a_ref) | copy-start | bytes 786436
  112.1 28.2 %collective-permute-start.18 = (bf16[4096,128]{1,0:T(8,128)(2,1)}, bf16[4096,128]{1,0:T(8,128)(2,1)}, u32[]{:S(2)}, u32[]{:S(2)}) collective-permute-start(bf16[4096,128]{1,0:T(8,128)(2,1)} %slice.18), channel_id=1, source_target_pairs={{0,2},{2,4},{4,6},{6,8},{8,10},{10,12},{12,14},{14,0},{1,3},{3,5},... | collective-permute-start | bytes 3145736 | tf_op jit(solution)/shard_map/ppermute | solution.py:555
  112.1 28.2 %collective-permute-start.19 = (bf16[4096,128]{1,0:T(8,128)(2,1)}, bf16[4096,128]{1,0:T(8,128)(2,1)S(1)}, u32[]{:S(2)}, u32[]{:S(2)}) collective-permute-start(bf16[4096,128]{1,0:T(8,128)(2,1)} %slice.19), channel_id=1, source_target_pairs={{0,14},{2,0},{4,2},{6,4},{8,6},{10,8},{12,10},{14,12},{1,15},{3,1}... | collective-permute-start | bytes 3145736 | tf_op jit(solution)/shard_map/ppermute | solution.py:555
  114.9 1.8 copy-start.6
  115.8 0.8 copy-start
  123.2 17.1 %copy-start.1 = (bf16[512,512]{1,0:T(8,128)(2,1)S(1)}, bf16[512,512]{1,0:T(8,128)(2,1)}, u32[]{:S(2)}) copy-start(bf16[512,512]{1,0:T(8,128)(2,1)} %copy-done) | copy-start | bytes 1572868
  123.2 17.1 %all-to-all-start.1 = ((bf16[16,160,128]{2,1,0:T(8,128)(2,1)}), bf16[16,160,128]{2,1,0:T(8,128)(2,1)}, u32[]{:S(2)}, u32[]{:S(2)}) async-start(bf16[16,160,128]{2,1,0:T(8,128)(2,1)} %get-tuple-element.64), calls=%async_computation.1 | async-start | bytes 1310720 | tf_op jit(solution)/shard_map/all_to_all | solution.py:648
  130.3 17.6 %collective-permute-start.22 = (bf16[2048,128]{1,0:T(8,128)(2,1)}, bf16[2048,128]{1,0:T(8,128)(2,1)}, u32[]{:S(2)}, u32[]{:S(2)}) collective-permute-start(bf16[2048,128]{1,0:T(8,128)(2,1)} %slice.21), channel_id=1, source_target_pairs={{0,2},{2,4},{4,6},{6,8},{8,10},{10,12},{12,14},{14,0},{1,3},{3,5},... | collective-permute-start | bytes 1572872 | tf_op jit(solution)/shard_map/ppermute | solution.py:555
  141.8 8.5 %copy-start.2 = (bf16[3,2048,128]{2,1,0:T(8,128)(2,1)S(1)}, bf16[3,2048,128]{2,1,0:T(8,128)(2,1)}, u32[]{:S(2)}) copy-start(bf16[3,2048,128]{2,1,0:T(8,128)(2,1)} %bundle.1) | copy-start | bytes 4718596
  141.9 8.5 %collective-permute-start.20 = (bf16[160,2048]{1,0:T(8,128)(2,1)S(1)}, bf16[160,2048]{1,0:T(8,128)(2,1)S(1)}, u32[]{:S(2)}, u32[]{:S(2)}) collective-permute-start(bf16[160,2048]{1,0:T(8,128)(2,1)S(1)} %rows_in.1.own_ref), channel_id=1, source_target_pairs={{0,1},{1,0},{2,3},{3,2},{4,5},{5,4},{6,7},{7,6},{8,9},{9,8},{10,11... | collective-permute-start | bytes 1966088 | tf_op jit(solution)/shard_map/ppermute | solution.py:568
  145.1 27.6 %collective-permute-start.25 = (bf16[2560,128]{1,0:T(8,128)(2,1)S(1)}, bf16[2560,128]{1,0:T(8,128)(2,1)S(1)}, u32[]{:S(2)}, u32[]{:S(2)}) collective-permute-start(bf16[2560,128]{1,0:T(8,128)(2,1)S(1)} %slice.23), channel_id=1, source_target_pairs={{0,14},{2,0},{4,2},{6,4},{8,6},{10,8},{12,10},{14,12},{1,15},{3,1}... | collective-permute-start | bytes 1966088 | tf_op jit(solution)/shard_map/ppermute | solution.py:555
  146.3 26.4 %collective-permute-start.21 = (bf16[2048,128]{1,0:T(8,128)(2,1)S(1)}, bf16[2048,128]{1,0:T(8,128)(2,1)S(1)}, u32[]{:S(2)}, u32[]{:S(2)}) collective-permute-start(bf16[2048,128]{1,0:T(8,128)(2,1)S(1)} %slice.20), channel_id=1, source_target_pairs={{0,14},{2,0},{4,2},{6,4},{8,6},{10,8},{12,10},{14,12},{1,15},{3,1}... | collective-permute-start | bytes 1572872 | tf_op jit(solution)/shard_map/ppermute | solution.py:555
  147.9 24.8 %collective-permute-start.23 = (bf16[2048,128]{1,0:T(8,128)(2,1)}, bf16[2048,128]{1,0:T(8,128)(2,1)S(1)}, u32[]{:S(2)}, u32[]{:S(2)}) collective-permute-start(bf16[2048,128]{1,0:T(8,128)(2,1)} %collective-permute-done.22.refs_5_), channel_id=1, source_target_pairs={{0,2},{2,4},{4,6},{6,8},{8,10},{10,12},{12,14},{14,0},{1,3},{3,5},... | collective-permute-start | bytes 1572872 | tf_op jit(solution)/shard_map/ppermute | solution.py:555
  148.9 23.8 %collective-permute-start.24 = (bf16[1536,128]{1,0:T(8,128)(2,1)S(1)}, bf16[1536,128]{1,0:T(8,128)(2,1)S(1)}, u32[]{:S(2)}, u32[]{:S(2)}) collective-permute-start(bf16[1536,128]{1,0:T(8,128)(2,1)S(1)} %slice.22), channel_id=1, source_target_pairs={{0,2},{2,4},{4,6},{6,8},{8,10},{10,12},{12,14},{14,0},{1,3},{3,5},... | collective-permute-start | bytes 1179656 | tf_op jit(solution)/shard_map/ppermute | solution.py:555
  174.0 2.7 %collective-permute-start.26 = (bf16[160,2048]{1,0:T(8,128)(2,1)S(1)}, bf16[160,2048]{1,0:T(8,128)(2,1)S(1)}, u32[]{:S(2)}, u32[]{:S(2)}) collective-permute-start(bf16[160,2048]{1,0:T(8,128)(2,1)S(1)} %get-tuple-element.69), channel_id=1, source_target_pairs={{0,1},{1,0},{2,3},{3,2},{4,5},{5,4},{6,7},{7,6},{8,9},{9,8},{10,11... | collective-permute-start | bytes 1966088 | tf_op jit(solution)/shard_map/ppermute | solution.py:568
  176.7 17.1 %copy-start.7 = (bf16[64,2048]{1,0:T(8,128)(2,1)S(1)}, bf16[64,2048]{1,0:T(8,128)(2,1)}, u32[]{:S(2)}) copy-start(bf16[64,2048]{1,0:T(8,128)(2,1)} %get-tuple-element.70.upd_ref) | copy-start | bytes 786436
